TPU v7x, 512 devices: a 4x2x32 block of a 4x8x32 slice. The times are simulated.
512 devices in a mesh: grp: 2 (over y), sp: 32 (over z), tp: 8 (over x, core).
Axes of the slice: x: 4, y: 2, z: 32, core: 2. Of those that a mesh axis runs over, the one named last changes fastest.
The devices are a block of a 4x8x32 slice.
Arguments:
- prompt: bfloat16 [8, 6144, 2048], P('grp', 'sp'), parts along dimension 0, may hold values from -6 to 6
- w_key: bfloat16 [2048, 2048], P('sp', 'tp'), may hold values from -0.125 to 0.125
- w_value: bfloat16 [2048, 2048], P('sp', 'tp'), may hold values from -0.125 to 0.125
- query_new: bfloat16 [8, 2048], P('grp', 'tp'), parts along dimension 0, may hold values from -150 to 150
- key_new: bfloat16 [8, 2048], P('grp', 'tp'), parts along dimension 0, may hold values from -15 to 15
- value_new: bfloat16 [8, 2048], P('grp', 'tp'), parts along dimension 0, may hold values from -6 to 6
- mix_lambda: float32 [16], P('tp'), may hold values from 0.3 to 0.8
- head_gain: float32 [128], replicated, may hold values from 0.1 to 1.9
Outputs:
- key_cache: bfloat16 [64, 32, 24, 2048], P(('grp', 'sp'), None, None, 'tp'), parts along dimension 0
- value_cache: bfloat16 [64, 32, 24, 2048], P(('grp', 'sp'), None, None, 'tp'), parts along dimension 0
- first_read: bfloat16 [8, 2048], P('grp', 'tp'), parts along dimension 0
There are 2 independent parts, one for each index of `grp`. A program takes and returns all parts, laid end to end along the dimension named above; an argument that names none is the same for every part. Nothing has to cross between parts.
All inputs are finite; a program needn't handle non-finite values.
Results may differ from a plain program's by a relative error of at most 0.0065.
The roundings to bfloat16 on the way count: a program that leaves them out, or rounds other values in their place, can miss the bound.
Values may be sent and summed in bfloat16 or wider, within the bound.
No kernel may reach another device: no remote copies, remote signals or barrier semaphores. Data moves between devices by JAX's collectives and lax.ppermute only.
A program may use at most 64 MiB of HBM per device.

v0:
```python
import jax
import jax.numpy as jnp
from jax import lax
from jax.sharding import PartitionSpec as P

HALF = 64
VDIM = 128


def sent_together(arrays, axis, dim, along):
    both = jnp.concatenate(arrays, axis=along)
    result, at, finished = (lax.all_gather(both, axis, axis=dim, tiled=True), 0, [])
    for a in arrays:
        finished.append(lax.slice_in_dim(result, at, at + a.shape[along], axis=along))
        at += a.shape[along]
    return tuple(finished)


def copy_for_each(shard, axis):
    peers = lax.axis_size(axis)
    return lax.all_to_all(
        jnp.broadcast_to(shard[None], (peers, *shard.shape)), axis, 0, 0, tiled=True
    )


def collected_together(shard, axis):
    leaves = jax.tree.leaves(shard)
    order = sorted(range(len(leaves)), key=lambda k: -leaves[k].size)
    width = (1, *leaves[order[0]].shape)[-1]
    lines = [
        jnp.pad(leaves[k].reshape(-1), (0, -leaves[k].size % width)).reshape(-1, width)
        for k in order
    ]
    both, at, found = (copy_for_each(jnp.concatenate(lines), axis), 0, {})
    for k, line in zip(order, lines):
        section = both[:, at : at + len(line)].reshape(len(both), -1)
        found[k] = section[:, : leaves[k].size].reshape(-1, *leaves[k].shape)
        at += len(line)
    numbers = iter(range(len(leaves)))
    return jax.tree.map(lambda _: found[next(numbers)], shard)


def combined_pairwise(pieces, combine):
    while len(jax.tree.leaves(pieces)[0]) > 1:
        pieces = jax.vmap(combine)(
            *(jax.tree.map(lambda part: part[side::2], pieces) for side in (0, 1))
        )
    return jax.tree.map(lambda part: part[0], pieces)


def merged(shard, axis, combine):
    pieces = collected_together(shard, axis)
    return combined_pairwise(pieces, combine)


def of_everyone(shard, axis):
    return copy_for_each(shard, axis).sum(axis=0)


def project(rows, w_key, w_value):
    pieces = sent_together((w_key, w_value), "sp", 0, 1)
    keys = jnp.dot(rows, pieces[0], preferred_element_type=jnp.float32)
    values = jnp.dot(rows, pieces[1], preferred_element_type=jnp.float32)
    return (keys.astype(jnp.bfloat16), values.astype(jnp.bfloat16))


def score_maps(query, keys):
    count, span = (keys.shape[0], keys.shape[1])
    heads = query.shape[1] // (2 * HALF)
    q_parts = query.reshape(count, heads, 2, HALF)
    k_parts = keys.reshape(count, span, heads, 2, HALF)
    return jnp.einsum(
        "shmc,slhmc->shml", q_parts, k_parts, preferred_element_type=jnp.float32
    ) * HALF ** (-0.5)


def own_scores(query, fresh_key):
    count = query.shape[0]
    heads = query.shape[1] // (2 * HALF)
    q_parts = query.astype(jnp.float32).reshape(count, heads, 2, HALF)
    k_parts = fresh_key.astype(jnp.float32).reshape(count, heads, 2, HALF)
    return jnp.sum(q_parts * k_parts, axis=-1) * HALF ** (-0.5)


def finish(reads, head_gain):
    mean = jnp.mean(reads * reads, axis=-1, keepdims=True)
    normed = reads * lax.rsqrt(mean + 1e-06) * head_gain
    return normed.reshape(reads.shape[0], -1).astype(jnp.bfloat16)


def join_totals(first, second):
    top = jnp.maximum(first[0], second[0])
    return (top, first[1] * jnp.exp(first[0] - top) + second[1] * jnp.exp(second[0] - top))


def placed(part_rows, prompts, first, fill):
    base = jnp.full((prompts,) + part_rows.shape[1:], fill, jnp.float32)
    return lax.dynamic_update_slice_in_dim(base, part_rows, first, 0)


def cache_read(query_new, key_new, value_new, keys, values, mix_lambda, head_gain, first):
    count, span = (keys.shape[0], keys.shape[1])
    prompts = query_new.shape[0]
    heads = mix_lambda.shape[0]
    query = lax.dynamic_slice_in_dim(query_new, first, count, 0)
    scores = score_maps(query, keys)
    fresh_all = own_scores(query_new, key_new)
    fresh = lax.dynamic_slice_in_dim(fresh_all, first, count, 0)
    local_top = jnp.maximum(jnp.max(scores, axis=-1), fresh)
    local_total = jnp.sum(jnp.exp(scores - local_top[..., None]), axis=-1)
    top_all, cache_total = merged(
        (placed(local_top, prompts, first, -1e30), placed(local_total, prompts, first, 0.0)),
        "sp",
        join_totals,
    )
    own = jnp.exp(fresh_all - top_all)
    total_all = cache_total + own
    top = lax.dynamic_slice_in_dim(top_all, first, count, 0)
    total = lax.dynamic_slice_in_dim(total_all, first, count, 0)
    probs = jnp.exp(scores - top[..., None]) / total[..., None]
    mixed = (probs[:, :, 0] - mix_lambda[None, :, None] * probs[:, :, 1]).astype(jnp.bfloat16)
    value_parts = values.reshape(count, span, heads, VDIM)
    partial_value = jnp.einsum(
        "shl,slhv->shv", mixed, value_parts, preferred_element_type=jnp.float32
    )
    reads = of_everyone(placed(partial_value, prompts, first, 0.0), "sp")
    own_prob = own / total_all
    own_mixed = (own_prob[:, :, 0] - mix_lambda[None, :] * own_prob[:, :, 1]).astype(jnp.bfloat16)
    reads = reads + own_mixed.astype(jnp.float32)[..., None] * value_new.astype(
        jnp.float32
    ).reshape(prompts, heads, VDIM)
    return finish(reads, head_gain)


def block_read(
    query_new, key_new, value_new, key_cache, value_cache, mix_lambda, head_gain, spread
):
    blocks, sub = (key_cache.shape[1], key_cache.shape[2])
    first = lax.axis_index("sp") // spread
    keys = key_cache.reshape(1, blocks * sub, -1)
    values = value_cache.reshape(1, blocks * sub, -1)
    return cache_read(query_new, key_new, value_new, keys, values, mix_lambda, head_gain, first)


def body(prompt, w_key, w_value, query_new, key_new, value_new, mix_lambda, head_gain):
    count, piece, width = prompt.shape
    spread = lax.axis_size("sp") // count
    sub = piece // spread
    keys, values = project(prompt.reshape(count * piece, width), w_key, w_value)
    key_blocks = keys.reshape(count * spread, 1, sub, -1)
    value_blocks = values.reshape(count * spread, 1, sub, -1)
    key_cache, value_cache = (
        lax.all_to_all(key_blocks, "sp", split_axis=0, concat_axis=1, tiled=True),
        lax.all_to_all(value_blocks, "sp", split_axis=0, concat_axis=1, tiled=True),
    )
    first_read = block_read(
        query_new, key_new, value_new, key_cache, value_cache, mix_lambda, head_gain, spread
    )
    return (key_cache, value_cache, first_read)


def solution(mesh):
    placed = (
        P("grp", "sp", None),
        P("sp", "tp"),
        P("sp", "tp"),
        P("grp", "tp"),
        P("grp", "tp"),
        P("grp", "tp"),
        P("tp"),
        P(),
    )
    return jax.shard_map(
        body,
        mesh=mesh,
        in_specs=placed,
        out_specs=(
            P(("grp", "sp"), None, None, "tp"),
            P(("grp", "sp"), None, None, "tp"),
            P("grp", "tp"),
        ),
        check_vma=False,
    )
```

profile of v0, /device:TPU:34, one launch (start us, length us, event | category | flops | bytes accessed | tf_op | source)
XLA Modules:
  0.0 364.4 jit_solution(18418636442365662421)
XLA Ops:
  7.3 1.6 pad_maximum_fusion
  8.9 164.9 %all-gather.2.cloned.1.call-done = bf16[2048,512]{1,0:T(8,128)(2,1)} async-done(((bf16[64,512]{1,0:T(8,128)(2,1)}), bf16[2048,512]{1,0:T(8,128)(2,1)}) %all-gather.2.cloned.1.call-update) | async-done | bytes 2097168 | tf_op jit(solution)/shard_map/all_gather | solution.py:12
  173.8 2.3 fusion
  177.0 11.1 %all-to-all-start = ((bf16[32,1,24,256]{3,2,1,0:T(8,128)(2,1)}), bf16[32,1,24,256]{3,2,1,0:T(8,128)(2,1)S(1)}, u32[]{:S(2)}, u32[]{:S(2)}) async-start(bf16[32,1,24,256]{3,2,1,0:T(8,128)(2,1)} %bitcast.90), calls=%async_computation | async-start | bytes 786432 | tf_op jit(solution)/shard_map/all_to_all | solution.py:153
  188.1 3.0 fusion.1
  191.1 1.9 copy.104
  193.1 32.8 %all-to-all-done = bf16[32,1,24,256]{3,2,1,0:T(8,128)(2,1)S(1)} async-done(((bf16[32,1,24,256]{3,2,1,0:T(8,128)(2,1)}), bf16[32,1,24,256]{3,2,1,0:T(8,128)(2,1)S(1)}, u32[]{:S(2)}, u32[]{:S(2)}) %all-to-all-start) | async-done | bytes 393248 | tf_op jit(solution)/shard_map/all_to_all | solution.py:153
  225.8 5.4 %all-to-all-start.1 = ((bf16[32,1,24,256]{3,2,1,0:T(8,128)(2,1)}), bf16[32,1,24,256]{3,2,1,0:T(8,128)(2,1)}, u32[]{:S(2)}, u32[]{:S(2)}) async-start(bf16[32,1,24,256]{3,2,1,0:T(8,128)(2,1)} %bitcast.89), calls=%async_computation.1 | async-start | bytes 786432 | tf_op jit(solution)/shard_map/all_to_all | solution.py:154
  234.1 1.5 fusion.4
  236.2 1.3 copy.107
  237.5 1.3 dynamic-slice_maximum_fusion
  240.2 1.3 copy.108
  243.4 1.3 reshape.124
  244.8 1.4 exponential_reduce_fusion
  252.1 17.1 %all-to-all-done.1 = bf16[32,1,24,256]{3,2,1,0:T(8,128)(2,1)} async-done(((bf16[32,1,24,256]{3,2,1,0:T(8,128)(2,1)}), bf16[32,1,24,256]{3,2,1,0:T(8,128)(2,1)}, u32[]{:S(2)}, u32[]{:S(2)}) %all-to-all-start.1) | async-done | bytes 393248 | tf_op jit(solution)/shard_map/all_to_all | solution.py:154
  270.4 5.3 %all-to-all-start.2 = ((f32[32,16,2]{1,2,0:T(2,128)}), f32[32,16,2]{1,2,0:T(2,128)}, u32[]{:S(2)}, u32[]{:S(2)}) async-start(f32[32,16,2]{1,2,0:T(2,128)} %broadcast_in_dim.9), calls=%async_computation.2 | async-start | bytes 65536 | tf_op jit(solution)/shard_map/all_to_all | solution.py:21
  275.8 1.8 reshape.126
  277.6 20.6 %all-to-all-done.2 = f32[32,16,2]{1,2,0:T(2,128)} async-done(((f32[32,16,2]{1,2,0:T(2,128)}), f32[32,16,2]{1,2,0:T(2,128)}, u32[]{:S(2)}, u32[]{:S(2)}) %all-to-all-start.2) | async-done | bytes 4128 | tf_op jit(solution)/shard_map/all_to_all | solution.py:21
  298.2 1.5 fusion.23
  299.7 1.4 copy.131
  301.1 1.5 slice.91
  302.6 1.5 slice.92
  304.1 1.4 copy.134
  305.5 1.5 slice.102
  307.0 1.5 slice.103
  308.5 1.4 copy.136
  309.9 1.4 copy.135
  311.3 1.4 copy.133
  312.7 1.4 copy.132
  320.5 5.4 %all-to-all-start.3 = ((f32[32,4,2,128]{3,2,1,0:T(2,128)}), f32[32,4,2,128]{3,2,1,0:T(2,128)}, u32[]{:S(2)}, u32[]{:S(2)}) async-start(f32[32,4,2,128]{3,2,1,0:T(2,128)} %broadcast_in_dim.11), calls=%async_computation.3 | async-start | bytes 262144 | tf_op jit(solution)/shard_map/all_to_all | solution.py:21
  328.1 24.5 %all-to-all-done.3 = f32[32,4,2,128]{3,2,1,0:T(2,128)} async-done(((f32[32,4,2,128]{3,2,1,0:T(2,128)}), f32[32,4,2,128]{3,2,1,0:T(2,128)}, u32[]{:S(2)}, u32[]{:S(2)}) %all-to-all-start.3) | async-done | bytes 131104 | tf_op jit(solution)/shard_map/all_to_all | solution.py:21
  355.8 1.8 copy.185
  (53 shorter events, 26.7 us)
Async XLA Ops:
  7.2 166.6 %copy-start = (bf16[4,192,2048]{2,1,0:T(8,128)(2,1)S(1)}, bf16[4,192,2048]{2,1,0:T(8,128)(2,1)}, u32[]{:S(2)}) copy-start(bf16[4,192,2048]{2,1,0:T(8,128)(2,1)} %param.8) | copy-start | bytes 9437188
  7.2 166.6 %all-gather.2.cloned.1.call-start = ((), (), s32[]{:S(2)}) async-start(), calls=%async_computation.4 | async-start | bytes 2162688 | tf_op jit(solution)/shard_map/all_gather | solution.py:12
  177.0 48.9 %all-to-all-start = ((bf16[32,1,24,256]{3,2,1,0:T(8,128)(2,1)}), bf16[32,1,24,256]{3,2,1,0:T(8,128)(2,1)S(1)}, u32[]{:S(2)}, u32[]{:S(2)}) async-start(bf16[32,1,24,256]{3,2,1,0:T(8,128)(2,1)} %bitcast.90), calls=%async_computation | async-start | bytes 786432 | tf_op jit(solution)/shard_map/all_to_all | solution.py:153
  188.1 43.2 %copy-start.1 = (bf16[4,256]{1,0:T(4,128)(2,1)S(1)}, bf16[4,256]{1,0:T(4,128)(2,1)}, u32[]{:S(2)}) copy-start(bf16[4,256]{1,0:T(4,128)(2,1)} %param.11) | copy-start | bytes 6148
  188.1 43.8 %copy-start.2 = (bf16[4,256]{1,0:T(4,128)(2,1)S(1)}, bf16[4,256]{1,0:T(4,128)(2,1)}, u32[]{:S(2)}) copy-start(bf16[4,256]{1,0:T(4,128)(2,1)} %param.12) | copy-start | bytes 6148
  225.8 43.3 %all-to-all-start.1 = ((bf16[32,1,24,256]{3,2,1,0:T(8,128)(2,1)}), bf16[32,1,24,256]{3,2,1,0:T(8,128)(2,1)}, u32[]{:S(2)}, u32[]{:S(2)}) async-start(bf16[32,1,24,256]{3,2,1,0:T(8,128)(2,1)} %bitcast.89), calls=%async_computation.1 | async-start | bytes 786432 | tf_op jit(solution)/shard_map/all_to_all | solution.py:154
  270.4 27.7 %all-to-all-start.2 = ((f32[32,16,2]{1,2,0:T(2,128)}), f32[32,16,2]{1,2,0:T(2,128)}, u32[]{:S(2)}, u32[]{:S(2)}) async-start(f32[32,16,2]{1,2,0:T(2,128)} %broadcast_in_dim.9), calls=%async_computation.2 | async-start | bytes 65536 | tf_op jit(solution)/shard_map/all_to_all | solution.py:21
  320.5 32.1 %all-to-all-start.3 = ((f32[32,4,2,128]{3,2,1,0:T(2,128)}), f32[32,4,2,128]{3,2,1,0:T(2,128)}, u32[]{:S(2)}, u32[]{:S(2)}) async-start(f32[32,4,2,128]{3,2,1,0:T(2,128)} %broadcast_in_dim.11), calls=%async_computation.3 | async-start | bytes 262144 | tf_op jit(solution)/shard_map/all_to_all | solution.py:21
Sparse Core Ops, SparseCore 0:
  10.7 163.0 all-gather.1
where the time goes:
time: 366 us; the launch traced here: 364 us
  waiting for transfers between devices  260 us (71%)
  local copies, waits for them, and re-layouts  42 us (11%)
  starting transfers between devices  27.3 us (7%)
  between operations  14.2 us (4%)
  other arithmetic  13.2 us (4%)
  matrix products  7.87 us (2%)
    all_gather x1, waiting for transfers between devices, sent_together(): lax.all_gather(both, axis, axis=dim, tiled=True)  165 us
    all_to_all x2, waiting for transfers between devices, copy_for_each(): lax.all_to_all(jnp.broadcast_to(shard[None], (peers, *shard.shape)), axis...  45 us
    all_to_all x1, waiting for transfers between devices, body(): lax.all_to_all(key_blocks, 'sp', split_axis=0, concat_axis=1, tiled=True)  32.8 us
    all_to_all x1, waiting for transfers between devices, body(): lax.all_to_all(value_blocks, 'sp', split_axis=0, concat_axis=1, tiled=True)  17.1 us
    all_to_all x1, starting transfers between devices, body(): lax.all_to_all(key_blocks, 'sp', split_axis=0, concat_axis=1, tiled=True)  11.1 us
    unnamed x15, local copies, waits for them, and re-layouts  11 us
    all_to_all x2, starting transfers between devices, copy_for_each(): lax.all_to_all(jnp.broadcast_to(shard[None], (peers, *shard.shape)), axis...  10.7 us
  transfers between devices with their start and end apart: 5, of which 5 were waited for; matrix products, arithmetic and copies ran while one was open for 8% of the time, Pallas kernels for 0%

commit v1 on v0

v1 whole, which is shorter than its diff:
```python
import functools
import jax
import jax.numpy as jnp
from jax import lax
from jax.experimental import pallas as pl
from jax.experimental.pallas import tpu as pltpu
from jax.sharding import PartitionSpec as P

HALF = 64
VDIM = 128
W_SHIFT = 2.0**18
X_SHIFT = 2.0**13
F32 = jnp.float32
BF16 = jnp.bfloat16
NEG = -1e30


def row_dot(a, b, precision=None):
    return lax.dot_general(a, b, (((1,), (1,)), ((), ())), preferred_element_type=F32, precision=precision)


def select_rows(rows, query, count, heads, pairs):
    width = query.shape[1]
    r = lax.broadcasted_iota(jnp.int32, (rows, width), 0)
    lane = lax.broadcasted_iota(jnp.int32, (rows, width), 1)
    out = jnp.zeros((rows, width), F32)
    for b in range(count):
        q = jnp.broadcast_to(query[b : b + 1, :].astype(F32), (rows, width))
        out = jnp.where((r // heads) % count == b, q, out)
    slot = (r % heads) * pairs + r // (count * heads)
    return jnp.where(lane // HALF == slot, out, 0.0)


def local_kernel(peers, heads, x_ref, w_ref, q_ref, scores_ref, v_ref, stats_ref):
    count, piece, width = x_ref.shape
    rows = 2 * count * heads
    cols = heads * 2 * HALF
    x = x_ref[...].reshape(count * piece, width)
    keys = jnp.dot(x, w_ref[:, :cols], preferred_element_type=F32).astype(BF16)
    v_ref[...] = jnp.dot(x, w_ref[:, cols:], preferred_element_type=F32).astype(BF16)
    picked = select_rows(rows, q_ref[...], count, heads, 2)
    scores = row_dot(picked.astype(BF16), keys) * HALF**-0.5
    r = lax.broadcasted_iota(jnp.int32, scores.shape, 0)
    at = lax.broadcasted_iota(jnp.int32, scores.shape, 1)
    scores = jnp.where((r // heads) % count == at // piece, scores, NEG)
    scores_ref[...] = scores
    top = jnp.max(scores, axis=1, keepdims=True)
    total = jnp.sum(jnp.exp(scores - top), axis=1, keepdims=True)
    both = jnp.concatenate([top, total, jnp.zeros((128 - 2 * rows, 1), F32)], axis=0)
    stats_ref[...] = jnp.broadcast_to(both, (128, 128)).T[:peers]


def merged(stats, query, fresh_key, count, heads):
    rows = 2 * count * heads
    by_row = stats.T
    tops = by_row[:rows]
    totals = by_row[rows : 2 * rows]
    fresh = select_rows(rows, query, count, heads, 2) * select_rows(rows, fresh_key, count, heads, 2)
    fresh = jnp.sum(fresh, axis=1, keepdims=True) * HALF**-0.5
    top = jnp.maximum(jnp.max(tops, axis=1, keepdims=True), fresh)
    own = jnp.exp(fresh - top)
    total = jnp.sum(totals * jnp.exp(tops - top), axis=1, keepdims=True) + own
    return top, total, own


def per_row(lam_ref, rows, heads):
    r = lax.broadcasted_iota(jnp.int32, (rows, 1), 0) % heads
    out = jnp.zeros((rows, 1), F32)
    for h in range(heads):
        out = jnp.where(r == h, lam_ref[h], out)
    return out


def read_kernel(peers, heads, lam_ref, scores_ref, v_ref, stats_ref, q_ref, kn_ref, part_ref, own_ref):
    count = q_ref.shape[0]
    half = count * heads
    top, total, own = merged(stats_ref[...], q_ref[...], kn_ref[...], count, heads)
    probs = jnp.exp(scores_ref[...] - top) / total
    lam = per_row(lam_ref, half, heads)
    mixed = (probs[:half] - lam * probs[half:]).astype(BF16)
    full = jnp.dot(mixed, v_ref[...], preferred_element_type=F32)
    r = lax.broadcasted_iota(jnp.int32, (half, VDIM), 0)
    part = jnp.zeros((half, VDIM), F32)
    for h in range(heads):
        part = jnp.where(r % heads == h, full[:, h * VDIM : (h + 1) * VDIM], part)
    for p in range(peers):
        part_ref[p] = part
    prob = own / total
    mine = (prob[:half] - lam * prob[half:]).astype(BF16).astype(F32)
    own_ref[...] = jnp.broadcast_to(mine, (half, VDIM))


def finish_kernel(heads, parts_ref, own_ref, vn_ref, gain_ref, out_ref):
    count = vn_ref.shape[0]
    half = count * heads
    reads = jnp.sum(parts_ref[...], axis=0)
    values = vn_ref[...].astype(F32)
    r = lax.broadcasted_iota(jnp.int32, (half, VDIM), 0)
    fresh = jnp.zeros((half, VDIM), F32)
    for b in range(count):
        for h in range(heads):
            row = jnp.broadcast_to(values[b : b + 1, h * VDIM : (h + 1) * VDIM], (half, VDIM))
            fresh = jnp.where(r == b * heads + h, row, fresh)
    reads = reads + own_ref[...] * fresh
    mean = jnp.mean(reads * reads, axis=1, keepdims=True)
    normed = reads * lax.rsqrt(mean + 1e-06) * gain_ref[...]
    for b in range(count):
        for h in range(heads):
            out_ref[b : b + 1, h * VDIM : (h + 1) * VDIM] = normed[b * heads + h : b * heads + h + 1].astype(BF16)


def block_kernel(x_ref, w_ref, k_ref, v_ref):
    slices, rows, depth = x_ref.shape
    cols = k_ref.shape[1]
    acc = jnp.zeros((rows, 2 * cols), F32)
    for t in range(slices):
        acc += jnp.dot(x_ref[t], w_ref[t * depth : (t + 1) * depth, :], preferred_element_type=F32)
    k_ref[...] = acc[:, :cols].astype(BF16)
    v_ref[...] = acc[:, cols:].astype(BF16)


def vmem(n):
    return [pl.BlockSpec(memory_space=pltpu.VMEM)] * n


def call(kernel, outs, args, smem=0):
    specs = [pl.BlockSpec(memory_space=pltpu.SMEM)] * smem + vmem(len(args) - smem)
    return pl.pallas_call(
        kernel,
        out_shape=[jax.ShapeDtypeStruct(s, d) for s, d in outs],
        in_specs=specs,
        out_specs=vmem(len(outs)),
        compiler_params=pltpu.CompilerParams(vmem_limit_bytes=40 << 20),
    )(*args)


def spread(x, axis):
    return lax.all_to_all(x, axis, 0, 0, tiled=True)


def body(prompt, w_key, w_value, query_new, key_new, value_new, mix_lambda, head_gain):
    count, piece, width = prompt.shape
    peers = lax.axis_size("sp")
    slices = lax.axis_size("tp")
    groups = peers // count
    sub = piece // groups
    heads = mix_lambda.shape[0]
    cols = w_key.shape[1]
    half = count * heads

    depth = width // slices
    mine = lax.dynamic_slice_in_dim(prompt, lax.axis_index("tp") * depth, depth, 2)
    mine = (mine.astype(F32) * X_SHIFT).astype(jnp.float16).reshape(peers, sub, depth)

    w = jnp.concatenate([w_key, w_value], axis=1)
    w = (w.astype(F32) * W_SHIFT).astype(jnp.float16)
    w = lax.all_gather(w, "sp", axis=0, tiled=True)
    w, mine = lax.optimization_barrier((w, mine))
    blocks = spread(mine, "sp")
    w = (w.astype(F32) * (1 / W_SHIFT)).astype(BF16)

    scores, values, stats = call(
        functools.partial(local_kernel, peers, heads),
        [((2 * half, count * piece), F32), ((count * piece, cols), BF16), ((peers, 128), F32)],
        (prompt, w, query_new),
    )
    stats = spread(stats, "sp")
    parts, own = call(
        functools.partial(read_kernel, peers, heads),
        [((peers, half, VDIM), F32), ((half, VDIM), F32)],
        (mix_lambda, scores, values, stats, query_new, key_new),
        smem=1,
    )
    parts = spread(parts, "sp")
    (first_read,) = call(
        functools.partial(finish_kernel, heads),
        [((count, cols), BF16)],
        (parts, own, value_new, head_gain.reshape(1, VDIM)),
    )

    blocks = lax.all_gather(blocks.reshape(peers * sub, depth), "tp", axis=0)
    blocks = (blocks.astype(F32) * (1 / X_SHIFT)).astype(BF16)
    key_cache, value_cache = call(
        block_kernel,
        [((peers * sub, cols), BF16)] * 2,
        (blocks, w),
    )
    shape = (1, peers, sub, cols)
    return key_cache.reshape(shape), value_cache.reshape(shape), first_read


def solution(mesh):
    return jax.shard_map(
        body,
        mesh=mesh,
        in_specs=(
            P("grp", "sp", None),
            P("sp", "tp"),
            P("sp", "tp"),
            P("grp", "tp"),
            P("grp", "tp"),
            P("grp", "tp"),
            P("tp"),
            P(),
        ),
        out_specs=(
            P(("grp", "sp"), None, None, "tp"),
            P(("grp", "sp"), None, None, "tp"),
            P("grp", "tp"),
        ),
        check_vma=False,
    )
```

time: 366 us -> 247 us (0.67)
  the two profiles are of different devices: /device:TPU:34 before, /device:TPU:33 now
where the time goes in v1:
time: 247 us
  blocking collectives  192 us (78%)
  waiting for transfers between devices  35.9 us (15%)
  Pallas kernels  6.43 us (3%)
  other arithmetic  5.36 us (2%)
  starting transfers between devices  4.79 us (2%)
    all_gather x1, blocking collectives, body(): w = lax.all_gather(w, 'sp', axis=0, tiled=True)  99.2 us
    all_to_all x2, blocking collectives, spread(): return lax.all_to_all(x, axis, 0, 0, tiled=True)  55.7 us
    all_gather x1, blocking collectives, body(): blocks = lax.all_gather(blocks.reshape(peers * sub, depth), 'tp', axis=0)  37 us
    all_to_all x1, waiting for transfers between devices, spread(): return lax.all_to_all(x, axis, 0, 0, tiled=True)  35.9 us
    pallas_call x4, Pallas kernels, call(): pl.pallas_call(kernel, out_shape=[jax.ShapeDtypeStruct(s, d) for s, d in...  6.43 us
  transfers between devices with their start and end apart: 1, of which 1 were waited for; matrix products, arithmetic and copies ran while one was open for 0% of the time, Pallas kernels for 0%

profile of v1, /device:TPU:33, one launch (start us, length us, event | category | flops | bytes accessed | tf_op | source)
XLA Modules:
  0.0 247.0 jit_solution(9783886578422914316)
XLA Ops:
  0.6 0.8 multiply_convert_fusion.3
  1.4 0.0 copy-start.1
  1.4 99.2 %all-gather.2 = f16[2048,512]{1,0:T(8,128)(2,1)} all-gather(f16[64,512]{1,0:T(8,128)(2,1)S(1)} %multiply_convert_fusion.3), channel_id=1, replica_groups=mesh['grp'=2,'sp'=32,'tp'=8] {'sp'}, dimensions={0}, use_global_device_ids=true | all-gather | bytes 2162688 | tf_op jit(solution)/shard_map/all_gather | solution.py:157
  100.7 1.8 multiply_convert_fusion.2
  102.5 2.0 multiply_convert_fusion.1.w_ref
  104.6 0.0 copy-done.1
  104.6 0.0 copy-start
  104.6 1.9 copy-done
  106.5 0.0 copy-start.2
  106.5 0.0 copy-start.5
  106.5 0.0 copy-start.3
  106.5 0.0 copy-start.4
  106.5 2.1 shard_map.104
  108.6 26.4 %all_to_all.21 = f32[32,1,128]{2,1,0:T(1,128)S(1)} all-to-all(f32[32,1,128]{2,1,0:T(1,128)S(1)} %bitcast.10), channel_id=1, replica_groups=mesh['grp'=2,'sp'=32,'tp'=8] {'sp'}, dimensions={0} | all-to-all | bytes 32768 | tf_op jit(solution)/shard_map/all_to_all | solution.py:138
  135.0 0.0 copy-done.2
  135.0 0.0 copy-done.5
  135.0 0.9 shard_map.105
  135.9 29.3 %all_to_all.22.parts_ref = f32[32,8,128]{2,1,0:T(8,128)S(1)} all-to-all(f32[32,8,128]{2,1,0:T(8,128)S(1)} %get-tuple-element.19), channel_id=1, replica_groups=mesh['grp'=2,'sp'=32,'tp'=8] {'sp'}, dimensions={0} | all-to-all | bytes 262144 | tf_op jit(solution)/shard_map/all_to_all | solution.py:138
  165.2 4.8 %all-to-all-start = ((f16[32,24,256]{2,1,0:T(8,128)(2,1)}), f16[32,24,256]{2,1,0:T(8,128)(2,1)S(1)}, u32[]{:S(2)}, u32[]{:S(2)}) async-start(f16[32,24,256]{2,1,0:T(8,128)(2,1)} %bitcast), calls=%async_computation | async-start | bytes 786432 | tf_op jit(solution)/shard_map/all_to_all | solution.py:138
  170.0 0.0 copy-done.3
  170.0 0.0 copy-done.4
  170.1 0.7 shard_map.106
  170.8 35.9 %all-to-all-done = f16[32,24,256]{2,1,0:T(8,128)(2,1)S(1)} async-done(((f16[32,24,256]{2,1,0:T(8,128)(2,1)}), f16[32,24,256]{2,1,0:T(8,128)(2,1)S(1)}, u32[]{:S(2)}, u32[]{:S(2)}) %all-to-all-start) | async-done | bytes 393248 | tf_op jit(solution)/shard_map/all_to_all | solution.py:138
  206.7 37.0 %all-gather.3 = f16[8,768,256]{2,1,0:T(8,128)(2,1)S(1)} all-gather(f16[1,768,256]{2,1,0:T(8,128)(2,1)S(1)} %bitcast.12), channel_id=1, replica_groups=mesh['grp'=2,'sp'=32,'tp'=8] {'tp'}, dimensions={0}, use_global_device_ids=true | all-gather | bytes 3538944 | tf_op jit(solution)/shard_map/all_gather | solution.py:181
  243.6 0.7 multiply_convert_fusion.x_ref
  244.3 2.7 %shard_map.103 = (bf16[768,256]{1,0:T(8,128)(2,1)}, bf16[768,256]{1,0:T(8,128)(2,1)}) custom-call(bf16[8,768,256]{2,1,0:T(8,128)(2,1)S(1)} %multiply_convert_fusion.x_ref, bf16[2048,512]{1,0:T(8,128)(2,1)S(1)} %multiply_convert_fusion.1.w_ref), custom_call_target="tpu_custom_call" | custom-call | tf_op jit(solution)/shard_map/pallas_call | solution.py:128
Async XLA Ops:
  1.4 103.1 %copy-start.1 = (bf16[4,256]{1,0:T(4,128)(2,1)S(1)}, bf16[4,256]{1,0:T(4,128)(2,1)}, u32[]{:S(2)}) copy-start(bf16[4,256]{1,0:T(4,128)(2,1)} %q_ref.3) | copy-start | bytes 6148
  104.6 1.9 copy-start
  106.5 28.5 %copy-start.2 = (bf16[4,256]{1,0:T(4,128)(2,1)S(1)}, bf16[4,256]{1,0:T(4,128)(2,1)}, u32[]{:S(2)}) copy-start(bf16[4,256]{1,0:T(4,128)(2,1)} %kn_ref.1) | copy-start | bytes 6148
  106.5 28.5 %copy-start.5 = (f32[2]{0:T(128)S(1)}, f32[2]{0:T(128)}, u32[]{:S(2)}) copy-start(f32[2]{0:T(128)} %lam_ref.1) | copy-start | bytes 28
  106.5 63.6 %copy-start.3 = (bf16[4,256]{1,0:T(4,128)(2,1)S(1)}, bf16[4,256]{1,0:T(4,128)(2,1)}, u32[]{:S(2)}) copy-start(bf16[4,256]{1,0:T(4,128)(2,1)} %vn_ref.1) | copy-start | bytes 6148
  106.5 63.6 %copy-start.4 = (f32[128]{0:T(128)S(1)}, f32[128]{0:T(128)}, u32[]{:S(2)}) copy-start(f32[128]{0:T(128)} %param.15) | copy-start | bytes 1540
  165.2 41.4 %all-to-all-start = ((f16[32,24,256]{2,1,0:T(8,128)(2,1)}), f16[32,24,256]{2,1,0:T(8,128)(2,1)S(1)}, u32[]{:S(2)}, u32[]{:S(2)}) async-start(f16[32,24,256]{2,1,0:T(8,128)(2,1)} %bitcast), calls=%async_computation | async-start | bytes 786432 | tf_op jit(solution)/shard_map/all_to_all | solution.py:138

commit v2 on v1

v2 whole, which is shorter than its diff:
```python
import functools
import jax
import jax.numpy as jnp
from jax import lax
from jax.experimental import pallas as pl
from jax.experimental.pallas import tpu as pltpu
from jax.sharding import PartitionSpec as P

HALF = 64
VDIM = 128
W_SHIFT = 2.0**18
F32 = jnp.float32
BF16 = jnp.bfloat16
NEG = -1e30
LIMIT = 16


def row_dot(a, b, precision=None):
    return lax.dot_general(a, b, (((1,), (1,)), ((), ())), preferred_element_type=F32, precision=precision)


def select_rows(rows, query, count, heads, pairs):
    width = query.shape[1]
    r = lax.broadcasted_iota(jnp.int32, (rows, width), 0)
    lane = lax.broadcasted_iota(jnp.int32, (rows, width), 1)
    out = jnp.zeros((rows, width), F32)
    for b in range(count):
        q = jnp.broadcast_to(query[b : b + 1, :].astype(F32), (rows, width))
        out = jnp.where((r // heads) % count == b, q, out)
    slot = (r % heads) * pairs + r // (count * heads)
    return jnp.where(lane // HALF == slot, out, 0.0)


def local_kernel(peers, heads, x_ref, w_ref, q_ref, part_ref):
    count, piece, width = x_ref.shape
    rows = 2 * count * heads
    cols = heads * 2 * HALF
    x = x_ref[...].reshape(count * piece, width)
    keys = jnp.dot(x, w_ref[:, :cols], preferred_element_type=F32).astype(BF16)
    values = jnp.dot(x, w_ref[:, cols:], preferred_element_type=F32).astype(BF16)
    picked = select_rows(rows, q_ref[...], count, heads, 2)
    scores = row_dot(picked.astype(BF16), keys) * HALF**-0.5
    r = lax.broadcasted_iota(jnp.int32, scores.shape, 0)
    at = lax.broadcasted_iota(jnp.int32, scores.shape, 1)
    scores = jnp.where((r // heads) % count == at // piece, scores, NEG)
    top = jnp.max(scores, axis=1, keepdims=True)
    weights = jnp.exp(scores - top)
    total = jnp.sum(weights, axis=1, keepdims=True)
    full = 0.0
    for p in three(weights):
        full += jnp.dot(p, values, preferred_element_type=F32)
    r = lax.broadcasted_iota(jnp.int32, (rows, VDIM), 0)
    part = jnp.zeros((rows, VDIM), F32)
    for h in range(heads):
        part = jnp.where(r % heads == h, full[:, h * VDIM : (h + 1) * VDIM], part)
    stats = as_line([top, total])
    for p in range(peers):
        part_ref[p * (rows + 1) : p * (rows + 1) + rows, :] = part
        part_ref[p * (rows + 1) + rows : (p + 1) * (rows + 1), :] = stats


def three(x):
    high = x.astype(BF16)
    rest = x - high.astype(F32)
    middle = rest.astype(BF16)
    return high, middle, (rest - middle.astype(F32)).astype(BF16)


def as_line(columns):
    rows = sum(c.shape[0] for c in columns)
    both = jnp.concatenate([*columns, jnp.zeros((VDIM - rows, 1), F32)], axis=0)
    return jnp.broadcast_to(both, (VDIM, VDIM)).T[:1]


def finish_kernel(peers, heads, lam_ref, part_ref, q_ref, kn_ref, vn_ref, gain_ref, out_ref):
    count = vn_ref.shape[0]
    half = count * heads
    rows = 2 * half
    fresh = select_rows(rows, q_ref[...], count, heads, 2) * select_rows(rows, kn_ref[...], count, heads, 2)
    fresh = as_line([jnp.sum(fresh, axis=1, keepdims=True) * HALF**-0.5])
    tops = part_ref[pl.ds(rows, peers, rows + 1), :]
    totals = pltpu.roll(tops, VDIM - rows, 1)
    top = jnp.maximum(jnp.max(tops, axis=0, keepdims=True), fresh)
    scale = jnp.exp(tops - top)
    own = jnp.exp(fresh - top)
    total = jnp.sum(totals * scale, axis=0, keepdims=True) + own
    lane = lax.broadcasted_iota(jnp.int32, (1, VDIM), 1)
    sign = jnp.ones((1, VDIM), F32)
    for h in range(heads):
        sign = jnp.where((lane >= half) & (lane % heads == h), -lam_ref[h], sign)
    scale = scale * (sign / total)
    own = own * (sign / total)
    mine = (own + pltpu.roll(own, VDIM - half, 1)).astype(BF16).astype(F32)
    values = vn_ref[...].astype(F32)
    for b in range(count):
        for h in range(heads):
            n = b * heads + h
            reads = 0.0
            for r in (n, n + half):
                reads += scale[:, r : r + 1] * part_ref[pl.ds(r, peers, rows + 1), :]
            reads = jnp.sum(reads, axis=0, keepdims=True)
            reads += mine[:, n : n + 1] * values[b : b + 1, h * VDIM : (h + 1) * VDIM]
            mean = jnp.mean(reads * reads, axis=1, keepdims=True)
            normed = reads * lax.rsqrt(mean + 1e-06) * gain_ref[...]
            out_ref[b : b + 1, h * VDIM : (h + 1) * VDIM] = normed.astype(BF16)


def block_kernel(slices, t_ref, *refs):
    x_refs, (w_ref, k_ref, v_ref, w_buf, sem) = refs[:slices], refs[slices:]
    rows, depth = x_refs[0].shape
    cols = k_ref.shape[1]
    moves = []
    for n in range(slices):
        w = pl.ds(pl.multiple_of(t_ref[n] * depth, depth), depth)
        moves.append(pltpu.make_async_copy(w_ref.at[w, :], w_buf.at[n], sem.at[n]))
        moves[n].start()
    step = rows // 4
    for at in range(0, rows, step):
        acc = 0.0
        for n in range(slices):
            if at == 0:
                moves[n].wait()
            acc += jnp.dot(x_refs[n][at : at + step, :], w_buf[n], preferred_element_type=F32)
        k_ref[at : at + step, :] = acc[:, :cols].astype(BF16)
        v_ref[at : at + step, :] = acc[:, cols:].astype(BF16)


def vmem(n):
    return [pl.BlockSpec(memory_space=pltpu.VMEM)] * n


def call(kernel, outs, args, spaces="", scratch=(), limit=16):
    kinds = {"s": pltpu.SMEM, "a": pl.ANY, "v": pltpu.VMEM}
    spaces = spaces.ljust(len(args), "v")
    return pl.pallas_call(
        kernel,
        out_shape=[jax.ShapeDtypeStruct(s, d) for s, d in outs],
        in_specs=[pl.BlockSpec(memory_space=kinds[c]) for c in spaces],
        out_specs=vmem(len(outs)),
        scratch_shapes=scratch,
        compiler_params=pltpu.CompilerParams(vmem_limit_bytes=int(limit * 2**20)),
    )(*args)


def spread(x, axis):
    return lax.all_to_all(x, axis, 0, 0, tiled=True)


def moved(x, axis, step):
    n = lax.axis_size(axis)
    return lax.ppermute(x, axis, [(i, step(i) % n) for i in range(n)])


def inner(prompt, w_key, w_value, query_new, key_new, value_new, mix_lambda, head_gain):
    count, piece, width = prompt.shape
    peers = lax.axis_size("sp")
    slices = lax.axis_size("tp")
    groups = peers // count
    sub = piece // groups
    heads = mix_lambda.shape[0]
    cols = w_key.shape[1]
    half = count * heads
    t = lax.axis_index("tp")

    depth = width // slices
    mine = lax.dynamic_slice_in_dim(prompt, t * depth, depth, 2).reshape(peers, sub, depth)
    w = jnp.concatenate([w_key, w_value], axis=1)
    w = (w.astype(F32) * W_SHIFT).astype(jnp.float16)
    mine, w = lax.optimization_barrier((mine, w))
    w = lax.all_gather(w, "sp", axis=0, tiled=True)
    w, mine = lax.optimization_barrier((w, mine))
    mine = spread(mine, "sp").reshape(peers * sub, depth)
    w = (w.astype(F32) * (1 / W_SHIFT)).astype(BF16)

    (parts,) = call(
        functools.partial(local_kernel, peers, heads), [((peers * (2 * half + 1), VDIM), F32)], (prompt, w, query_new)
    )
    parts = parts.reshape(peers, 1, (2 * half + 1) * VDIM)
    parts = spread(parts, "sp").reshape(peers * (2 * half + 1), VDIM)
    (first_read,) = call(
        functools.partial(finish_kernel, peers, heads),
        [((count, cols), BF16)],
        (mix_lambda, parts, query_new, key_new, value_new, head_gain.reshape(1, VDIM)),
        "s",
    )

    found, who = [mine], [t]
    for d in range(1, slices // 2):
        found.append(moved(mine, "tp", lambda i: i + 2 * d))
        who.append((t - 2 * d) % slices)
    for n in range(slices // 2):
        found.append(moved(found[n], "tp", lambda i: i ^ 1))
        who.append(who[n] ^ 1)
    key_cache, value_cache = call(
        functools.partial(block_kernel, slices),
        [((peers * sub, cols), BF16)] * 2,
        (jnp.stack(who), *found, w),
        "s" + "v" * slices + "a",
        [pltpu.VMEM((slices, depth, 2 * cols), BF16), pltpu.SemaphoreType.DMA((slices,))],
        LIMIT,
    )
    shape = (1, peers, sub, cols)
    return key_cache.reshape(shape), value_cache.reshape(shape), first_read


def solution(mesh):
    return jax.shard_map(
        inner,
        mesh=mesh,
        in_specs=(
            P("grp", "sp", None),
            P("sp", "tp"),
            P("sp", "tp"),
            P("grp", "tp"),
            P("grp", "tp"),
            P("grp", "tp"),
            P("tp"),
            P(),
        ),
        out_specs=(
            P(("grp", "sp"), None, None, "tp"),
            P(("grp", "sp"), None, None, "tp"),
            P("grp", "tp"),
        ),
        check_vma=False,
    )
```

time: 247 us -> 223 us (0.903)
  the two profiles are of different devices: /device:TPU:33 before, /device:TPU:40 now
where the time goes in v2:
time: 223 us; the launch traced here: 222 us
  blocking collectives  124 us (56%)
  waiting for transfers between devices  44.9 us (20%)
  starting transfers between devices  31.1 us (14%)
  Pallas kernels  9.53 us (4%)
  local copies, waits for them, and re-layouts  8.37 us (4%)
  other arithmetic  2.83 us (1%)
    all_gather x1, blocking collectives, inner(): w = lax.all_gather(w, 'sp', axis=0, tiled=True)  124 us
    all_to_all x2, waiting for transfers between devices, spread(): return lax.all_to_all(x, axis, 0, 0, tiled=True)  41.2 us
    ppermute x7, starting transfers between devices, moved(): return lax.ppermute(x, axis, [(i, step(i) % n) for i in range(n)])  18.8 us
    all_to_all x2, starting transfers between devices, spread(): return lax.all_to_all(x, axis, 0, 0, tiled=True)  12.3 us
    pallas_call x3, Pallas kernels, call(): pl.pallas_call(kernel, out_shape=[jax.ShapeDtypeStruct(s, d) for s, d in...  9.53 us
    unnamed x16, local copies, waits for them, and re-layouts  5.91 us
  transfers between devices with their start and end apart: 9, of which 4 were waited for; matrix products, arithmetic and copies ran while one was open for 1% of the time, Pallas kernels for 2%

profile of v2, /device:TPU:40, one launch (start us, length us, event | category | flops | bytes accessed | tf_op | source)
XLA Modules:
  0.0 221.8 jit_solution(6998359876507718577)
XLA Ops:
  0.6 0.8 multiply_convert_fusion.1
  1.4 1.8 constant_dynamic-slice_fusion
  3.2 124.2 %all-gather.1 = f16[2048,512]{1,0:T(8,128)(2,1)} all-gather(f16[64,512]{1,0:T(8,128)(2,1)S(1)} %multiply_convert_fusion.1), channel_id=1, replica_groups=mesh['grp'=2,'sp'=32,'tp'=8] {'sp'}, dimensions={0}, use_global_device_ids=true | all-gather | bytes 2162688 | tf_op jit(solution)/shard_map/all_gather | solution.py:170
  127.4 4.8 %all-to-all-start = ((bf16[32,24,256]{2,1,0:T(8,128)(2,1)}), bf16[32,24,256]{2,1,0:T(8,128)(2,1)S(1)}, u32[]{:S(2)}, u32[]{:S(2)}) async-start(bf16[32,24,256]{2,1,0:T(8,128)(2,1)} %bitcast.8), calls=%async_computation | async-start | bytes 786432 | tf_op jit(solution)/shard_map/all_to_all | solution.py:146
  132.2 2.0 multiply_convert_fusion.refs_8_.w_ref
  134.3 0.0 copy-start
  134.3 1.9 copy-done
  136.2 3.2 %shard_map.104 = f32[544,128]{1,0:T(8,128)} custom-call(bf16[4,192,2048]{2,1,0:T(8,128)(2,1)S(1)} %copy-done, bf16[2048,512]{1,0:T(8,128)(2,1)S(1)} %multiply_convert_fusion.refs_8_.w_ref, bf16[4,256]{1,0:T(4,128)(2,1)S(1)} %copy-done.1), custom_call_target="tpu_custom_call" | custom-call | tf_op jit(solution)/shard_map/pallas_call | solution.py:135
  139.3 31.7 %all-to-all-done = bf16[32,24,256]{2,1,0:T(8,128)(2,1)S(1)} async-done(((bf16[32,24,256]{2,1,0:T(8,128)(2,1)}), bf16[32,24,256]{2,1,0:T(8,128)(2,1)S(1)}, u32[]{:S(2)}, u32[]{:S(2)}) %all-to-all-start) | async-done | bytes 393248 | tf_op jit(solution)/shard_map/all_to_all | solution.py:146
  171.0 7.5 %all-to-all-start.1 = ((f32[32,1,2176]{2,1,0:T(1,128)}), f32[32,1,2176]{2,1,0:T(1,128)S(1)}, u32[]{:S(2)}, u32[]{:S(2)}) async-start(f32[32,1,2176]{2,1,0:T(1,128)} %bitcast.12), calls=%async_computation.1 | async-start | bytes 557056 | tf_op jit(solution)/shard_map/all_to_all | solution.py:146
  178.6 5.1 %collective-permute-start.2 = (bf16[768,256]{1,0:T(8,128)(2,1)S(1)}, bf16[768,256]{1,0:T(8,128)(2,1)S(1)}, u32[]{:S(2)}, u32[]{:S(2)}) collective-permute-start(bf16[768,256]{1,0:T(8,128)(2,1)S(1)} %bitcast.15), channel_id=1, source_target_pairs={{0,6},{1,7},{2,0},{3,1},{4,2},{5,3},{6,4},{7,5},{8,14},{9,15},{10,... | collective-permute-start | bytes 1179656 | tf_op jit(solution)/shard_map/ppermute | solution.py:151
  183.7 2.5 %collective-permute-start.1 = (bf16[768,256]{1,0:T(8,128)(2,1)S(1)}, bf16[768,256]{1,0:T(8,128)(2,1)S(1)}, u32[]{:S(2)}, u32[]{:S(2)}) collective-permute-start(bf16[768,256]{1,0:T(8,128)(2,1)S(1)} %bitcast.16), channel_id=1, source_target_pairs={{0,4},{1,5},{2,6},{3,7},{4,0},{5,1},{6,2},{7,3},{8,12},{9,13},{10,... | collective-permute-start | bytes 1179656 | tf_op jit(solution)/shard_map/ppermute | solution.py:151
  186.1 3.0 %collective-permute-start = (bf16[768,256]{1,0:T(8,128)(2,1)S(1)}, bf16[768,256]{1,0:T(8,128)(2,1)}, u32[]{:S(2)}, u32[]{:S(2)}) collective-permute-start(bf16[768,256]{1,0:T(8,128)(2,1)S(1)} %bitcast.17), channel_id=1, source_target_pairs={{0,2},{1,3},{2,4},{3,5},{4,6},{5,7},{6,0},{7,1},{8,10},{9,11},{10,... | collective-permute-start | bytes 1179656 | tf_op jit(solution)/shard_map/ppermute | solution.py:151
  189.1 2.0 collective-permute-start.3
  191.1 2.1 collective-permute-done.2.refs_3_
  193.2 1.9 collective-permute-start.6
  195.1 0.0 collective-permute-done.1.refs_2_
  195.1 2.4 %collective-permute-start.5 = (bf16[768,256]{1,0:T(8,128)(2,1)S(1)}, bf16[768,256]{1,0:T(8,128)(2,1)}, u32[]{:S(2)}, u32[]{:S(2)}) collective-permute-start(bf16[768,256]{1,0:T(8,128)(2,1)S(1)} %collective-permute-done.1.refs_2_), channel_id=1, source_target_pairs={{0,1},{1,0},{2,3},{3,2},{4,5},{5,4},{6,7},{7,6},{8,9},{9,8},{10,11... | collective-permute-start | bytes 1179656 | tf_op jit(solution)/shard_map/ppermute | solution.py:151
  197.6 1.6 collective-permute-done.refs_1_
  199.2 1.9 collective-permute-start.4
  201.2 0.7 stack.35.t_ref
  201.9 9.5 %all-to-all-done.1 = f32[32,1,2176]{2,1,0:T(1,128)S(1)} async-done(((f32[32,1,2176]{2,1,0:T(1,128)}), f32[32,1,2176]{2,1,0:T(1,128)S(1)}, u32[]{:S(2)}, u32[]{:S(2)}) %all-to-all-start.1) | async-done | bytes 278560 | tf_op jit(solution)/shard_map/all_to_all | solution.py:146
  211.4 0.7 copy-done.2
  212.1 0.7 copy-done.3
  212.8 0.7 copy-done.4
  213.4 0.7 copy-done.6
  214.1 0.7 copy-done.7
  214.8 1.6 shard_map.105
  216.4 0.0 collective-permute-done.3.refs_4_
  216.4 0.0 collective-permute-done.6.refs_7_
  216.4 0.7 copy-done.5
  217.1 4.7 %shard_map.103 = (bf16[768,256]{1,0:T(8,128)(2,1)}, bf16[768,256]{1,0:T(8,128)(2,1)}) custom-call(s32[8]{0:T(128)S(1)} %copy-done.5, bf16[768,256]{1,0:T(8,128)(2,1)S(1)} %bitcast.19, bf16[768,256]{1,0:T(8,128)(2,1)} %collective-permute-done.refs_1_, bf16[768,256]{1,0:T(8,128)(2,1)S(1)} %collective-permute-done.1.refs_2_, ...), custom_call_target="tpu_custom_call" | custom-call | tf_op jit(solution)/shard_map/pallas_call | solution.py:135
  (10 shorter events, 0.0 us)
Async XLA Ops:
  3.2 131.1 %copy-start.1 = (bf16[4,256]{1,0:T(4,128)(2,1)S(1)}, bf16[4,256]{1,0:T(4,128)(2,1)}, u32[]{:S(2)}) copy-start(bf16[4,256]{1,0:T(4,128)(2,1)} %q_ref.3) | copy-start | bytes 6148
  127.4 43.6 %all-to-all-start = ((bf16[32,24,256]{2,1,0:T(8,128)(2,1)}), bf16[32,24,256]{2,1,0:T(8,128)(2,1)S(1)}, u32[]{:S(2)}, u32[]{:S(2)}) async-start(bf16[32,24,256]{2,1,0:T(8,128)(2,1)} %bitcast.8), calls=%async_computation | async-start | bytes 786432 | tf_op jit(solution)/shard_map/all_to_all | solution.py:146
  134.3 1.9 copy-start
  171.0 40.4 %all-to-all-start.1 = ((f32[32,1,2176]{2,1,0:T(1,128)}), f32[32,1,2176]{2,1,0:T(1,128)S(1)}, u32[]{:S(2)}, u32[]{:S(2)}) async-start(f32[32,1,2176]{2,1,0:T(1,128)} %bitcast.12), calls=%async_computation.1 | async-start | bytes 557056 | tf_op jit(solution)/shard_map/all_to_all | solution.py:146
  178.6 14.6 %collective-permute-start.2 = (bf16[768,256]{1,0:T(8,128)(2,1)S(1)}, bf16[768,256]{1,0:T(8,128)(2,1)S(1)}, u32[]{:S(2)}, u32[]{:S(2)}) collective-permute-start(bf16[768,256]{1,0:T(8,128)(2,1)S(1)} %bitcast.15), channel_id=1, source_target_pairs={{0,6},{1,7},{2,0},{3,1},{4,2},{5,3},{6,4},{7,5},{8,14},{9,15},{10,... | collective-permute-start | bytes 1179656 | tf_op jit(solution)/shard_map/ppermute | solution.py:151
  183.7 11.5 %collective-permute-start.1 = (bf16[768,256]{1,0:T(8,128)(2,1)S(1)}, bf16[768,256]{1,0:T(8,128)(2,1)S(1)}, u32[]{:S(2)}, u32[]{:S(2)}) collective-permute-start(bf16[768,256]{1,0:T(8,128)(2,1)S(1)} %bitcast.16), channel_id=1, source_target_pairs={{0,4},{1,5},{2,6},{3,7},{4,0},{5,1},{6,2},{7,3},{8,12},{9,13},{10,... | collective-permute-start | bytes 1179656 | tf_op jit(solution)/shard_map/ppermute | solution.py:151
  186.1 13.0 %collective-permute-start = (bf16[768,256]{1,0:T(8,128)(2,1)S(1)}, bf16[768,256]{1,0:T(8,128)(2,1)}, u32[]{:S(2)}, u32[]{:S(2)}) collective-permute-start(bf16[768,256]{1,0:T(8,128)(2,1)S(1)} %bitcast.17), channel_id=1, source_target_pairs={{0,2},{1,3},{2,4},{3,5},{4,6},{5,7},{6,0},{7,1},{8,10},{9,11},{10,... | collective-permute-start | bytes 1179656 | tf_op jit(solution)/shard_map/ppermute | solution.py:151
  189.1 27.3 %collective-permute-start.3 = (bf16[768,256]{1,0:T(8,128)(2,1)S(1)}, bf16[768,256]{1,0:T(8,128)(2,1)}, u32[]{:S(2)}, u32[]{:S(2)}) collective-permute-start(bf16[768,256]{1,0:T(8,128)(2,1)S(1)} %bitcast.18), channel_id=1, source_target_pairs={{0,1},{1,0},{2,3},{3,2},{4,5},{5,4},{6,7},{7,6},{8,9},{9,8},{10,11... | collective-permute-start | bytes 1179656 | tf_op jit(solution)/shard_map/ppermute | solution.py:151
  193.2 23.2 %collective-permute-start.6 = (bf16[768,256]{1,0:T(8,128)(2,1)S(1)}, bf16[768,256]{1,0:T(8,128)(2,1)}, u32[]{:S(2)}, u32[]{:S(2)}) collective-permute-start(bf16[768,256]{1,0:T(8,128)(2,1)S(1)} %collective-permute-done.2.refs_3_), channel_id=1, source_target_pairs={{0,1},{1,0},{2,3},{3,2},{4,5},{5,4},{6,7},{7,6},{8,9},{9,8},{10,11... | collective-permute-start | bytes 1179656 | tf_op jit(solution)/shard_map/ppermute | solution.py:151
  195.1 21.3 %collective-permute-start.5 = (bf16[768,256]{1,0:T(8,128)(2,1)S(1)}, bf16[768,256]{1,0:T(8,128)(2,1)}, u32[]{:S(2)}, u32[]{:S(2)}) collective-permute-start(bf16[768,256]{1,0:T(8,128)(2,1)S(1)} %collective-permute-done.1.refs_2_), channel_id=1, source_target_pairs={{0,1},{1,0},{2,3},{3,2},{4,5},{5,4},{6,7},{7,6},{8,9},{9,8},{10,11... | collective-permute-start | bytes 1179656 | tf_op jit(solution)/shard_map/ppermute | solution.py:151
  199.2 17.2 %collective-permute-start.4 = (bf16[768,256]{1,0:T(8,128)(2,1)}, bf16[768,256]{1,0:T(8,128)(2,1)}, u32[]{:S(2)}, u32[]{:S(2)}) collective-permute-start(bf16[768,256]{1,0:T(8,128)(2,1)} %collective-permute-done.refs_1_), channel_id=1, source_target_pairs={{0,1},{1,0},{2,3},{3,2},{4,5},{5,4},{6,7},{7,6},{8,9},{9,8},{10,11... | collective-permute-start | bytes 1179656 | tf_op jit(solution)/shard_map/ppermute | solution.py:151
  211.4 0.7 copy-start.2
  212.1 0.7 copy-start.3
  212.8 0.7 copy-start.4
  213.4 0.7 copy-start.6
  214.1 0.7 copy-start.7
  216.4 0.7 copy-start.5

commit v3 on v2

--- a/solution.py
+++ b/solution.py
@@ -72,26 +72,40 @@
     return jnp.broadcast_to(both, (VDIM, VDIM)).T[:1]
 
 
-def finish_kernel(peers, heads, lam_ref, part_ref, q_ref, kn_ref, vn_ref, gain_ref, out_ref):
+def fresh_kernel(heads, lam_ref, q_ref, kn_ref, vn_ref, gain_ref, out_ref):
     count = vn_ref.shape[0]
     half = count * heads
     rows = 2 * half
     fresh = select_rows(rows, q_ref[...], count, heads, 2) * select_rows(rows, kn_ref[...], count, heads, 2)
-    fresh = as_line([jnp.sum(fresh, axis=1, keepdims=True) * HALF**-0.5])
+    out_ref[0:1, :] = as_line([jnp.sum(fresh, axis=1, keepdims=True) * HALF**-0.5])
+    lane = lax.broadcasted_iota(jnp.int32, (1, VDIM), 1)
+    sign = jnp.ones((1, VDIM), F32)
+    for h in range(heads):
+        sign = jnp.where((lane >= half) & (lane % heads == h), -lam_ref[h], sign)
+    out_ref[1:2, :] = sign
+    out_ref[2:3, :] = gain_ref[...]
+    out_ref[3:8, :] = jnp.zeros((5, VDIM), F32)
+    values = vn_ref[...].astype(F32)
+    for b in range(count):
+        for h in range(heads):
+            n = 8 + b * heads + h
+            out_ref[n : n + 1, :] = values[b : b + 1, h * VDIM : (h + 1) * VDIM]
+
+
+def finish_kernel(peers, heads, part_ref, new_ref, out_ref):
+    count = out_ref.shape[0]
+    half = count * heads
+    rows = 2 * half
+    fresh = new_ref[0:1, :]
     tops = part_ref[pl.ds(rows, peers, rows + 1), :]
     totals = pltpu.roll(tops, VDIM - rows, 1)
     top = jnp.maximum(jnp.max(tops, axis=0, keepdims=True), fresh)
     scale = jnp.exp(tops - top)
     own = jnp.exp(fresh - top)
     total = jnp.sum(totals * scale, axis=0, keepdims=True) + own
-    lane = lax.broadcasted_iota(jnp.int32, (1, VDIM), 1)
-    sign = jnp.ones((1, VDIM), F32)
-    for h in range(heads):
-        sign = jnp.where((lane >= half) & (lane % heads == h), -lam_ref[h], sign)
-    scale = scale * (sign / total)
-    own = own * (sign / total)
+    scale = scale * (new_ref[1:2, :] / total)
+    own = own * (new_ref[1:2, :] / total)
     mine = (own + pltpu.roll(own, VDIM - half, 1)).astype(BF16).astype(F32)
-    values = vn_ref[...].astype(F32)
     for b in range(count):
         for h in range(heads):
             n = b * heads + h
@@ -99,34 +113,40 @@
             for r in (n, n + half):
                 reads += scale[:, r : r + 1] * part_ref[pl.ds(r, peers, rows + 1), :]
             reads = jnp.sum(reads, axis=0, keepdims=True)
-            reads += mine[:, n : n + 1] * values[b : b + 1, h * VDIM : (h + 1) * VDIM]
+            reads += mine[:, n : n + 1] * new_ref[8 + n : 9 + n, :]
             mean = jnp.mean(reads * reads, axis=1, keepdims=True)
-            normed = reads * lax.rsqrt(mean + 1e-06) * gain_ref[...]
+            normed = reads * lax.rsqrt(mean + 1e-06) * new_ref[2:3, :]
             out_ref[b : b + 1, h * VDIM : (h + 1) * VDIM] = normed.astype(BF16)
 
 
-def block_kernel(slices, t_ref, *refs):
-    x_refs, (w_ref, k_ref, v_ref, w_buf, sem) = refs[:slices], refs[slices:]
+def block_kernel(slices, *refs):
+    x_refs, (w_ref, k_ref, v_ref, x_buf, w_buf, sem) = refs[:slices], refs[slices:]
     rows, depth = x_refs[0].shape
     cols = k_ref.shape[1]
+    t = lax.axis_index("tp")
+    who = [lax.rem(t + slices - 2 * d, slices) for d in range(slices // 2)]
+    who += [lax.bitwise_xor(n, 1) for n in who]
     moves = []
     for n in range(slices):
-        w = pl.ds(pl.multiple_of(t_ref[n] * depth, depth), depth)
-        moves.append(pltpu.make_async_copy(w_ref.at[w, :], w_buf.at[n], sem.at[n]))
-        moves[n].start()
+        w = pl.ds(pl.multiple_of(who[n] * depth, depth), depth)
+        moves.append(
+            [
+                pltpu.make_async_copy(w_ref.at[w, :], w_buf.at[n], sem.at[n, 0]),
+                pltpu.make_async_copy(x_refs[n], x_buf.at[n], sem.at[n, 1]),
+            ]
+        )
+        for m in moves[n]:
+            m.start()
     step = rows // 4
     for at in range(0, rows, step):
         acc = 0.0
         for n in range(slices):
             if at == 0:
-                moves[n].wait()
-            acc += jnp.dot(x_refs[n][at : at + step, :], w_buf[n], preferred_element_type=F32)
+                for m in moves[n]:
+                    m.wait()
+            acc += jnp.dot(x_buf[n, at : at + step, :], w_buf[n], preferred_element_type=F32)
         k_ref[at : at + step, :] = acc[:, :cols].astype(BF16)
         v_ref[at : at + step, :] = acc[:, cols:].astype(BF16)
-
-
-def vmem(n):
-    return [pl.BlockSpec(memory_space=pltpu.VMEM)] * n
 
 
 def call(kernel, outs, args, spaces="", scratch=(), limit=16):
@@ -136,7 +156,7 @@
         kernel,
         out_shape=[jax.ShapeDtypeStruct(s, d) for s, d in outs],
         in_specs=[pl.BlockSpec(memory_space=kinds[c]) for c in spaces],
-        out_specs=vmem(len(outs)),
+        out_specs=[pl.BlockSpec(memory_space=pltpu.VMEM)] * len(outs),
         scratch_shapes=scratch,
         compiler_params=pltpu.CompilerParams(vmem_limit_bytes=int(limit * 2**20)),
     )(*args)
@@ -168,35 +188,38 @@
     w = (w.astype(F32) * W_SHIFT).astype(jnp.float16)
     mine, w = lax.optimization_barrier((mine, w))
     w = lax.all_gather(w, "sp", axis=0, tiled=True)
+    w = (w.astype(F32) * (1 / W_SHIFT)).astype(BF16)
     w, mine = lax.optimization_barrier((w, mine))
     mine = spread(mine, "sp").reshape(peers * sub, depth)
-    w = (w.astype(F32) * (1 / W_SHIFT)).astype(BF16)
-
+
+    (fresh,) = call(
+        functools.partial(fresh_kernel, heads),
+        [((8 + half, VDIM), F32)],
+        (mix_lambda, query_new, key_new, value_new, head_gain.reshape(1, VDIM)),
+        "s",
+    )
     (parts,) = call(
         functools.partial(local_kernel, peers, heads), [((peers * (2 * half + 1), VDIM), F32)], (prompt, w, query_new)
     )
     parts = parts.reshape(peers, 1, (2 * half + 1) * VDIM)
     parts = spread(parts, "sp").reshape(peers * (2 * half + 1), VDIM)
-    (first_read,) = call(
-        functools.partial(finish_kernel, peers, heads),
-        [((count, cols), BF16)],
-        (mix_lambda, parts, query_new, key_new, value_new, head_gain.reshape(1, VDIM)),
-        "s",
-    )
-
-    found, who = [mine], [t]
+    (first_read,) = call(functools.partial(finish_kernel, peers, heads), [((count, cols), BF16)], (parts, fresh))
+
+    found = [mine]
     for d in range(1, slices // 2):
         found.append(moved(mine, "tp", lambda i: i + 2 * d))
-        who.append((t - 2 * d) % slices)
     for n in range(slices // 2):
         found.append(moved(found[n], "tp", lambda i: i ^ 1))
-        who.append(who[n] ^ 1)
     key_cache, value_cache = call(
         functools.partial(block_kernel, slices),
         [((peers * sub, cols), BF16)] * 2,
-        (jnp.stack(who), *found, w),
-        "s" + "v" * slices + "a",
-        [pltpu.VMEM((slices, depth, 2 * cols), BF16), pltpu.SemaphoreType.DMA((slices,))],
+        (*found, w),
+        "a" * (slices + 1),
+        [
+            pltpu.VMEM((slices, peers * sub, depth), BF16),
+            pltpu.VMEM((slices, depth, 2 * cols), BF16),
+            pltpu.SemaphoreType.DMA((slices, 2)),
+        ],
         LIMIT,
     )
     shape = (1, peers, sub, cols)

time: 223 us -> 213 us (0.955)
  blocking collectives: 124 us -> 120 us
  waiting for transfers between devices: 44.9 us -> 41.2 us
    all_gather x1, blocking collectives: 124 us -> 120 us  [inner(): w = lax.all_gather(w, 'sp', axis=0, tiled=True)]
    ppermute x7, waiting for transfers between devices: 3.73 us -> 0.35 us  [moved(): return lax.ppermute(x, axis, [(i, step(i) % n) for i in range(n)])]
    unnamed x16 -> x18, local copies, waits for them, and re-layouts: 5.91 us -> 6.56 us
    pallas_call x3 -> x4, Pallas kernels: 9.53 us -> 9.48 us  [call(): pl.pallas_call(kernel, out_shape=[jax.ShapeDtypeStruct(s, d) for s, d in...]
  transfers between devices with their start and end apart: 9 -> 9, of which waited for: 4 -> 3; matrix products, arithmetic and copies ran while one was open for 1% -> 0% of each run, Pallas kernels for 2% -> 2%
where the time goes in v3:
time: 213 us
  blocking collectives  120 us (56%)
  waiting for transfers between devices  41.2 us (19%)
  starting transfers between devices  31.7 us (15%)
  Pallas kernels  9.48 us (4%)
  local copies, waits for them, and re-layouts  8.33 us (4%)
    all_gather x1, blocking collectives, inner(): w = lax.all_gather(w, 'sp', axis=0, tiled=True)  120 us
    all_to_all x2, waiting for transfers between devices, spread(): return lax.all_to_all(x, axis, 0, 0, tiled=True)  40.8 us
    ppermute x7, starting transfers between devices, moved(): return lax.ppermute(x, axis, [(i, step(i) % n) for i in range(n)])  20.5 us
    all_to_all x2, starting transfers between devices, spread(): return lax.all_to_all(x, axis, 0, 0, tiled=True)  11.2 us
    pallas_call x4, Pallas kernels, call(): pl.pallas_call(kernel, out_shape=[jax.ShapeDtypeStruct(s, d) for s, d in...  9.48 us
    unnamed x18, local copies, waits for them, and re-layouts  6.56 us
  transfers between devices with their start and end apart: 9, of which 3 were waited for; matrix products, arithmetic and copies ran while one was open for 0% of the time, Pallas kernels for 2%

profile of v3, /device:TPU:40, one launch (start us, length us, event | category | flops | bytes accessed | tf_op | source)
XLA Modules:
  0.0 212.6 jit_solution(5576755582895336108)
XLA Ops:
  0.6 1.8 constant_dynamic-slice_fusion
  2.4 0.8 multiply_convert_fusion.1
  3.2 0.0 copy-start.3
  3.2 119.8 %all-gather.1 = f16[2048,512]{1,0:T(8,128)(2,1)S(1)} all-gather(f16[64,512]{1,0:T(8,128)(2,1)S(1)} %multiply_convert_fusion.1), channel_id=1, replica_groups=mesh['grp'=2,'sp'=32,'tp'=8] {'sp'}, dimensions={0}, use_global_device_ids=true | all-gather | bytes 2162688 | tf_op jit(solution)/shard_map/all_gather | solution.py:190
  123.0 0.5 multiply_convert_fusion.refs_8_.w_ref
  123.5 4.8 %all-to-all-start = ((bf16[32,24,256]{2,1,0:T(8,128)(2,1)}), bf16[32,24,256]{2,1,0:T(8,128)(2,1)S(1)}, u32[]{:S(2)}, u32[]{:S(2)}) async-start(bf16[32,24,256]{2,1,0:T(8,128)(2,1)} %bitcast), calls=%async_computation | async-start | bytes 786432 | tf_op jit(solution)/shard_map/all_to_all | solution.py:166
  128.3 0.0 copy-start
  128.3 1.9 copy-done
  130.2 3.2 %shard_map.104 = f32[544,128]{1,0:T(8,128)} custom-call(bf16[4,192,2048]{2,1,0:T(8,128)(2,1)S(1)} %copy-done, bf16[2048,512]{1,0:T(8,128)(2,1)S(1)} %multiply_convert_fusion.refs_8_.w_ref, bf16[4,256]{1,0:T(4,128)(2,1)S(1)} %copy-done.3), custom_call_target="tpu_custom_call" | custom-call | tf_op jit(solution)/shard_map/pallas_call | solution.py:155
  133.4 33.6 %all-to-all-done = bf16[32,24,256]{2,1,0:T(8,128)(2,1)S(1)} async-done(((bf16[32,24,256]{2,1,0:T(8,128)(2,1)}), bf16[32,24,256]{2,1,0:T(8,128)(2,1)S(1)}, u32[]{:S(2)}, u32[]{:S(2)}) %all-to-all-start) | async-done | bytes 393248 | tf_op jit(solution)/shard_map/all_to_all | solution.py:166
  167.0 6.4 %all-to-all-start.1 = ((f32[32,1,2176]{2,1,0:T(1,128)}), f32[32,1,2176]{2,1,0:T(1,128)S(1)}, u32[]{:S(2)}, u32[]{:S(2)}) async-start(f32[32,1,2176]{2,1,0:T(1,128)} %bitcast.4), calls=%async_computation.1 | async-start | bytes 557056 | tf_op jit(solution)/shard_map/all_to_all | solution.py:166
  173.5 3.6 %collective-permute-start = (bf16[768,256]{1,0:T(8,128)(2,1)S(1)}, bf16[768,256]{1,0:T(8,128)(2,1)S(1)}, u32[]{:S(2)}, u32[]{:S(2)}) collective-permute-start(bf16[768,256]{1,0:T(8,128)(2,1)S(1)} %bitcast.7), channel_id=1, source_target_pairs={{0,2},{1,3},{2,4},{3,5},{4,6},{5,7},{6,0},{7,1},{8,10},{9,11},{10,... | collective-permute-start | bytes 1179656 | tf_op jit(solution)/shard_map/ppermute | solution.py:171
  177.0 4.9 %collective-permute-start.1 = (bf16[768,256]{1,0:T(8,128)(2,1)S(1)}, bf16[768,256]{1,0:T(8,128)(2,1)S(1)}, u32[]{:S(2)}, u32[]{:S(2)}) collective-permute-start(bf16[768,256]{1,0:T(8,128)(2,1)S(1)} %bitcast.8), channel_id=1, source_target_pairs={{0,4},{1,5},{2,6},{3,7},{4,0},{5,1},{6,2},{7,3},{8,12},{9,13},{10,... | collective-permute-start | bytes 1179656 | tf_op jit(solution)/shard_map/ppermute | solution.py:171
  182.0 3.2 %collective-permute-start.2 = (bf16[768,256]{1,0:T(8,128)(2,1)S(1)}, bf16[768,256]{1,0:T(8,128)(2,1)}, u32[]{:S(2)}, u32[]{:S(2)}) collective-permute-start(bf16[768,256]{1,0:T(8,128)(2,1)S(1)} %bitcast.9), channel_id=1, source_target_pairs={{0,6},{1,7},{2,0},{3,1},{4,2},{5,3},{6,4},{7,5},{8,14},{9,15},{10,... | collective-permute-start | bytes 1179656 | tf_op jit(solution)/shard_map/ppermute | solution.py:171
  185.2 2.0 collective-permute-start.3
  187.2 0.0 collective-permute-done.refs_1_
  187.2 2.4 %collective-permute-start.4 = (bf16[768,256]{1,0:T(8,128)(2,1)S(1)}, bf16[768,256]{1,0:T(8,128)(2,1)}, u32[]{:S(2)}, u32[]{:S(2)}) collective-permute-start(bf16[768,256]{1,0:T(8,128)(2,1)S(1)} %collective-permute-done.refs_1_), channel_id=1, source_target_pairs={{0,1},{1,0},{2,3},{3,2},{4,5},{5,4},{6,7},{7,6},{8,9},{9,8},{10,11... | collective-permute-start | bytes 1179656 | tf_op jit(solution)/shard_map/ppermute | solution.py:171
  189.6 0.3 collective-permute-done.1.refs_2_
  190.0 1.9 collective-permute-start.5
  191.9 2.4 %collective-permute-start.6 = (bf16[768,256]{1,0:T(8,128)(2,1)}, bf16[768,256]{1,0:T(8,128)(2,1)}, u32[]{:S(2)}, u32[]{:S(2)}) collective-permute-start(bf16[768,256]{1,0:T(8,128)(2,1)} %collective-permute-done.2.refs_3_), channel_id=1, source_target_pairs={{0,1},{1,0},{2,3},{3,2},{4,5},{5,4},{6,7},{7,6},{8,9},{9,8},{10,11... | collective-permute-start | bytes 1179656 | tf_op jit(solution)/shard_map/ppermute | solution.py:171
  194.4 0.0 copy-start.4
  194.4 0.7 copy-done.4
  195.1 0.7 copy-done.5
  195.8 0.7 copy-done.6
  196.4 0.7 copy-done.7
  197.1 0.7 copy-done.8
  197.7 0.8 shard_map.105.new_ref
  198.5 0.6 copy-done.1
  199.1 7.2 %all-to-all-done.1 = f32[32,1,2176]{2,1,0:T(1,128)S(1)} async-done(((f32[32,1,2176]{2,1,0:T(1,128)}), f32[32,1,2176]{2,1,0:T(1,128)S(1)}, u32[]{:S(2)}, u32[]{:S(2)}) %all-to-all-start.1) | async-done | bytes 278560 | tf_op jit(solution)/shard_map/all_to_all | solution.py:166
  206.3 0.7 copy-done.2
  207.0 0.9 shard_map.106
  208.0 4.6 %shard_map.103 = (bf16[768,256]{1,0:T(8,128)(2,1)}, bf16[768,256]{1,0:T(8,128)(2,1)}) custom-call(bf16[768,256]{1,0:T(8,128)(2,1)S(1)} %bitcast.11, bf16[768,256]{1,0:T(8,128)(2,1)S(1)} %collective-permute-done.refs_1_, bf16[768,256]{1,0:T(8,128)(2,1)S(1)} %collective-permute-done.1.refs_2_, bf16[768,256]{1,0:T(8,128)(2,1)} %collective-permute-done.2.refs_3_, ...), custom_call_target="tpu_custom_call" | custom-call | tf_op jit(solution)/shard_map/pallas_call | solution.py:155
  (12 shorter events, 0.0 us)
Async XLA Ops:
  3.2 125.1 %copy-start.3 = (bf16[4,256]{1,0:T(4,128)(2,1)S(1)}, bf16[4,256]{1,0:T(4,128)(2,1)}, u32[]{:S(2)}) copy-start(bf16[4,256]{1,0:T(4,128)(2,1)} %q_ref.3) | copy-start | bytes 6148
  123.5 43.5 %all-to-all-start = ((bf16[32,24,256]{2,1,0:T(8,128)(2,1)}), bf16[32,24,256]{2,1,0:T(8,128)(2,1)S(1)}, u32[]{:S(2)}, u32[]{:S(2)}) async-start(bf16[32,24,256]{2,1,0:T(8,128)(2,1)} %bitcast), calls=%async_computation | async-start | bytes 786432 | tf_op jit(solution)/shard_map/all_to_all | solution.py:166
  128.3 1.9 copy-start
  167.0 39.3 %all-to-all-start.1 = ((f32[32,1,2176]{2,1,0:T(1,128)}), f32[32,1,2176]{2,1,0:T(1,128)S(1)}, u32[]{:S(2)}, u32[]{:S(2)}) async-start(f32[32,1,2176]{2,1,0:T(1,128)} %bitcast.4), calls=%async_computation.1 | async-start | bytes 557056 | tf_op jit(solution)/shard_map/all_to_all | solution.py:166
  173.5 13.7 %collective-permute-start = (bf16[768,256]{1,0:T(8,128)(2,1)S(1)}, bf16[768,256]{1,0:T(8,128)(2,1)S(1)}, u32[]{:S(2)}, u32[]{:S(2)}) collective-permute-start(bf16[768,256]{1,0:T(8,128)(2,1)S(1)} %bitcast.7), channel_id=1, source_target_pairs={{0,2},{1,3},{2,4},{3,5},{4,6},{5,7},{6,0},{7,1},{8,10},{9,11},{10,... | collective-permute-start | bytes 1179656 | tf_op jit(solution)/shard_map/ppermute | solution.py:171
  177.0 12.9 %collective-permute-start.1 = (bf16[768,256]{1,0:T(8,128)(2,1)S(1)}, bf16[768,256]{1,0:T(8,128)(2,1)S(1)}, u32[]{:S(2)}, u32[]{:S(2)}) collective-permute-start(bf16[768,256]{1,0:T(8,128)(2,1)S(1)} %bitcast.8), channel_id=1, source_target_pairs={{0,4},{1,5},{2,6},{3,7},{4,0},{5,1},{6,2},{7,3},{8,12},{9,13},{10,... | collective-permute-start | bytes 1179656 | tf_op jit(solution)/shard_map/ppermute | solution.py:171
  182.0 9.9 %collective-permute-start.2 = (bf16[768,256]{1,0:T(8,128)(2,1)S(1)}, bf16[768,256]{1,0:T(8,128)(2,1)}, u32[]{:S(2)}, u32[]{:S(2)}) collective-permute-start(bf16[768,256]{1,0:T(8,128)(2,1)S(1)} %bitcast.9), channel_id=1, source_target_pairs={{0,6},{1,7},{2,0},{3,1},{4,2},{5,3},{6,4},{7,5},{8,14},{9,15},{10,... | collective-permute-start | bytes 1179656 | tf_op jit(solution)/shard_map/ppermute | solution.py:171
  185.2 22.7 %collective-permute-start.3 = (bf16[768,256]{1,0:T(8,128)(2,1)S(1)}, bf16[768,256]{1,0:T(8,128)(2,1)}, u32[]{:S(2)}, u32[]{:S(2)}) collective-permute-start(bf16[768,256]{1,0:T(8,128)(2,1)S(1)} %bitcast.10), channel_id=1, source_target_pairs={{0,1},{1,0},{2,3},{3,2},{4,5},{5,4},{6,7},{7,6},{8,9},{9,8},{10,11... | collective-permute-start | bytes 1179656 | tf_op jit(solution)/shard_map/ppermute | solution.py:171
  187.2 20.7 %collective-permute-start.4 = (bf16[768,256]{1,0:T(8,128)(2,1)S(1)}, bf16[768,256]{1,0:T(8,128)(2,1)}, u32[]{:S(2)}, u32[]{:S(2)}) collective-permute-start(bf16[768,256]{1,0:T(8,128)(2,1)S(1)} %collective-permute-done.refs_1_), channel_id=1, source_target_pairs={{0,1},{1,0},{2,3},{3,2},{4,5},{5,4},{6,7},{7,6},{8,9},{9,8},{10,11... | collective-permute-start | bytes 1179656 | tf_op jit(solution)/shard_map/ppermute | solution.py:171
  190.0 18.0 %collective-permute-start.5 = (bf16[768,256]{1,0:T(8,128)(2,1)S(1)}, bf16[768,256]{1,0:T(8,128)(2,1)}, u32[]{:S(2)}, u32[]{:S(2)}) collective-permute-start(bf16[768,256]{1,0:T(8,128)(2,1)S(1)} %collective-permute-done.1.refs_2_), channel_id=1, source_target_pairs={{0,1},{1,0},{2,3},{3,2},{4,5},{5,4},{6,7},{7,6},{8,9},{9,8},{10,11... | collective-permute-start | bytes 1179656 | tf_op jit(solution)/shard_map/ppermute | solution.py:171
  191.9 16.0 %collective-permute-start.6 = (bf16[768,256]{1,0:T(8,128)(2,1)}, bf16[768,256]{1,0:T(8,128)(2,1)}, u32[]{:S(2)}, u32[]{:S(2)}) collective-permute-start(bf16[768,256]{1,0:T(8,128)(2,1)} %collective-permute-done.2.refs_3_), channel_id=1, source_target_pairs={{0,1},{1,0},{2,3},{3,2},{4,5},{5,4},{6,7},{7,6},{8,9},{9,8},{10,11... | collective-permute-start | bytes 1179656 | tf_op jit(solution)/shard_map/ppermute | solution.py:171
  194.4 0.7 copy-start.4
  195.1 0.7 copy-start.5
  195.7 0.7 copy-start.6
  196.4 0.7 copy-start.7
  197.1 0.7 copy-start.8
  198.5 0.6 copy-start.1
  206.3 0.7 copy-start.2

commit v4 on v3

--- a/solution.py
+++ b/solution.py
@@ -72,7 +72,7 @@
     return jnp.broadcast_to(both, (VDIM, VDIM)).T[:1]
 
 
-def fresh_kernel(heads, lam_ref, q_ref, kn_ref, vn_ref, gain_ref, out_ref):
+def fresh_kernel(heads, lam_ref, met_ref, q_ref, kn_ref, vn_ref, gain_ref, out_ref):
     count = vn_ref.shape[0]
     half = count * heads
     rows = 2 * half
@@ -190,13 +190,14 @@
     w = lax.all_gather(w, "sp", axis=0, tiled=True)
     w = (w.astype(F32) * (1 / W_SHIFT)).astype(BF16)
     w, mine = lax.optimization_barrier((w, mine))
+    met = moved(w[:8, :VDIM], "tp", lambda i: i ^ 1)
     mine = spread(mine, "sp").reshape(peers * sub, depth)
 
     (fresh,) = call(
         functools.partial(fresh_kernel, heads),
         [((8 + half, VDIM), F32)],
-        (mix_lambda, query_new, key_new, value_new, head_gain.reshape(1, VDIM)),
-        "s",
+        (mix_lambda, met, query_new, key_new, value_new, head_gain.reshape(1, VDIM)),
+        "sa",
     )
     (parts,) = call(
         functools.partial(local_kernel, peers, heads), [((peers * (2 * half + 1), VDIM), F32)], (prompt, w, query_new)

time: 213 us -> 213 us (level)
    all_to_all x2, waiting for transfers between devices: 40.8 us -> 37.7 us  [spread(): return lax.all_to_all(x, axis, 0, 0, tiled=True)]
    ppermute x7 -> x8, starting transfers between devices: 20.5 us -> 22.5 us  [moved(): return lax.ppermute(x, axis, [(i, step(i) % n) for i in range(n)])]
  transfers between devices with their start and end apart: 9 -> 10, of which waited for: 3 -> 4; matrix products, arithmetic and copies ran while one was open for 0% -> 0% of each run, Pallas kernels for 2% -> 2%
where the time goes in v4:
time: 213 us
  blocking collectives  120 us (56%)
  waiting for transfers between devices  39.2 us (18%)
  starting transfers between devices  33.7 us (16%)
  Pallas kernels  9.48 us (4%)
  local copies, waits for them, and re-layouts  8.33 us (4%)
    all_gather x1, blocking collectives, inner(): w = lax.all_gather(w, 'sp', axis=0, tiled=True)  120 us
    all_to_all x2, waiting for transfers between devices, spread(): return lax.all_to_all(x, axis, 0, 0, tiled=True)  37.7 us
    ppermute x8, starting transfers between devices, moved(): return lax.ppermute(x, axis, [(i, step(i) % n) for i in range(n)])  22.5 us
    all_to_all x2, starting transfers between devices, spread(): return lax.all_to_all(x, axis, 0, 0, tiled=True)  11.2 us
    pallas_call x4, Pallas kernels, call(): pl.pallas_call(kernel, out_shape=[jax.ShapeDtypeStruct(s, d) for s, d in...  9.48 us
    unnamed x18, local copies, waits for them, and re-layouts  6.56 us
  transfers between devices with their start and end apart: 10, of which 4 were waited for; matrix products, arithmetic and copies ran while one was open for 0% of the time, Pallas kernels for 2%

profile of v4, /device:TPU:40, one launch (start us, length us, event | category | flops | bytes accessed | tf_op | source)
XLA Modules:
  0.0 212.6 jit_solution(3876149314727937961)
XLA Ops:
  0.6 1.8 constant_dynamic-slice_fusion
  2.4 0.8 multiply_convert_fusion.1
  3.2 0.0 copy-start.3
  3.2 119.8 %all-gather.1 = f16[2048,512]{1,0:T(8,128)(2,1)S(1)} all-gather(f16[64,512]{1,0:T(8,128)(2,1)S(1)} %multiply_convert_fusion.1), channel_id=1, replica_groups=mesh['grp'=2,'sp'=32,'tp'=8] {'sp'}, dimensions={0}, use_global_device_ids=true | all-gather | bytes 2162688 | tf_op jit(solution)/shard_map/all_gather | solution.py:190
  123.0 0.5 multiply_convert_fusion.refs_8_.w_ref
  123.5 4.8 %all-to-all-start = ((bf16[32,24,256]{2,1,0:T(8,128)(2,1)}), bf16[32,24,256]{2,1,0:T(8,128)(2,1)S(1)}, u32[]{:S(2)}, u32[]{:S(2)}) async-start(bf16[32,24,256]{2,1,0:T(8,128)(2,1)} %bitcast), calls=%async_computation | async-start | bytes 786432 | tf_op jit(solution)/shard_map/all_to_all | solution.py:166
  128.3 0.0 copy-start
  128.3 1.9 copy-done
  130.2 3.2 %shard_map.104 = f32[544,128]{1,0:T(8,128)} custom-call(bf16[4,192,2048]{2,1,0:T(8,128)(2,1)S(1)} %copy-done, bf16[2048,512]{1,0:T(8,128)(2,1)S(1)} %multiply_convert_fusion.refs_8_.w_ref, bf16[4,256]{1,0:T(4,128)(2,1)S(1)} %copy-done.3), custom_call_target="tpu_custom_call" | custom-call | tf_op jit(solution)/shard_map/pallas_call | solution.py:155
  133.4 33.6 %all-to-all-done = bf16[32,24,256]{2,1,0:T(8,128)(2,1)S(1)} async-done(((bf16[32,24,256]{2,1,0:T(8,128)(2,1)}), bf16[32,24,256]{2,1,0:T(8,128)(2,1)S(1)}, u32[]{:S(2)}, u32[]{:S(2)}) %all-to-all-start) | async-done | bytes 393248 | tf_op jit(solution)/shard_map/all_to_all | solution.py:166
  167.0 6.4 %all-to-all-start.1 = ((f32[32,1,2176]{2,1,0:T(1,128)}), f32[32,1,2176]{2,1,0:T(1,128)S(1)}, u32[]{:S(2)}, u32[]{:S(2)}) async-start(f32[32,1,2176]{2,1,0:T(1,128)} %bitcast.4), calls=%async_computation.1 | async-start | bytes 557056 | tf_op jit(solution)/shard_map/all_to_all | solution.py:166
  173.5 3.6 %collective-permute-start = (bf16[768,256]{1,0:T(8,128)(2,1)S(1)}, bf16[768,256]{1,0:T(8,128)(2,1)S(1)}, u32[]{:S(2)}, u32[]{:S(2)}) collective-permute-start(bf16[768,256]{1,0:T(8,128)(2,1)S(1)} %bitcast.7), channel_id=1, source_target_pairs={{0,2},{1,3},{2,4},{3,5},{4,6},{5,7},{6,0},{7,1},{8,10},{9,11},{10,... | collective-permute-start | bytes 1179656 | tf_op jit(solution)/shard_map/ppermute | solution.py:171
  177.0 4.9 %collective-permute-start.1 = (bf16[768,256]{1,0:T(8,128)(2,1)S(1)}, bf16[768,256]{1,0:T(8,128)(2,1)S(1)}, u32[]{:S(2)}, u32[]{:S(2)}) collective-permute-start(bf16[768,256]{1,0:T(8,128)(2,1)S(1)} %bitcast.8), channel_id=1, source_target_pairs={{0,4},{1,5},{2,6},{3,7},{4,0},{5,1},{6,2},{7,3},{8,12},{9,13},{10,... | collective-permute-start | bytes 1179656 | tf_op jit(solution)/shard_map/ppermute | solution.py:171
  182.0 3.2 %collective-permute-start.2 = (bf16[768,256]{1,0:T(8,128)(2,1)S(1)}, bf16[768,256]{1,0:T(8,128)(2,1)}, u32[]{:S(2)}, u32[]{:S(2)}) collective-permute-start(bf16[768,256]{1,0:T(8,128)(2,1)S(1)} %bitcast.9), channel_id=1, source_target_pairs={{0,6},{1,7},{2,0},{3,1},{4,2},{5,3},{6,4},{7,5},{8,14},{9,15},{10,... | collective-permute-start | bytes 1179656 | tf_op jit(solution)/shard_map/ppermute | solution.py:171
  185.2 2.0 collective-permute-start.3
  187.2 2.4 %collective-permute-start.4 = (bf16[768,256]{1,0:T(8,128)(2,1)S(1)}, bf16[768,256]{1,0:T(8,128)(2,1)}, u32[]{:S(2)}, u32[]{:S(2)}) collective-permute-start(bf16[768,256]{1,0:T(8,128)(2,1)S(1)} %collective-permute-done.refs_1_), channel_id=1, source_target_pairs={{0,1},{1,0},{2,3},{3,2},{4,5},{5,4},{6,7},{7,6},{8,9},{9,8},{10,11... | collective-permute-start | bytes 1179656 | tf_op jit(solution)/shard_map/ppermute | solution.py:171
  189.6 0.3 collective-permute-done.1.refs_2_
  190.0 1.9 collective-permute-start.5
  191.9 2.4 %collective-permute-start.6 = (bf16[768,256]{1,0:T(8,128)(2,1)}, bf16[768,256]{1,0:T(8,128)(2,1)}, u32[]{:S(2)}, u32[]{:S(2)}) collective-permute-start(bf16[768,256]{1,0:T(8,128)(2,1)} %collective-permute-done.2.refs_3_), channel_id=1, source_target_pairs={{0,1},{1,0},{2,3},{3,2},{4,5},{5,4},{6,7},{7,6},{8,9},{9,8},{10,11... | collective-permute-start | bytes 1179656 | tf_op jit(solution)/shard_map/ppermute | solution.py:171
  194.4 2.0 collective-permute-start.7
  196.3 1.1 collective-permute-done.7.met_ref
  197.5 0.7 copy-done.4
  198.2 0.7 copy-done.5
  198.8 0.7 copy-done.6
  199.5 0.7 copy-done.7
  200.2 0.7 copy-done.8
  200.8 0.8 shard_map.105.new_ref
  201.6 0.6 copy-done.1
  202.2 4.1 %all-to-all-done.1 = f32[32,1,2176]{2,1,0:T(1,128)S(1)} async-done(((f32[32,1,2176]{2,1,0:T(1,128)}), f32[32,1,2176]{2,1,0:T(1,128)S(1)}, u32[]{:S(2)}, u32[]{:S(2)}) %all-to-all-start.1) | async-done | bytes 278560 | tf_op jit(solution)/shard_map/all_to_all | solution.py:166
  206.3 0.7 copy-done.2
  207.0 0.9 shard_map.106
  208.0 4.6 %shard_map.103 = (bf16[768,256]{1,0:T(8,128)(2,1)}, bf16[768,256]{1,0:T(8,128)(2,1)}) custom-call(bf16[768,256]{1,0:T(8,128)(2,1)S(1)} %bitcast.11, bf16[768,256]{1,0:T(8,128)(2,1)S(1)} %collective-permute-done.refs_1_, bf16[768,256]{1,0:T(8,128)(2,1)S(1)} %collective-permute-done.1.refs_2_, bf16[768,256]{1,0:T(8,128)(2,1)} %collective-permute-done.2.refs_3_, ...), custom_call_target="tpu_custom_call" | custom-call | tf_op jit(solution)/shard_map/pallas_call | solution.py:155
  (15 shorter events, 0.0 us)
Async XLA Ops:
  3.2 125.1 %copy-start.3 = (bf16[4,256]{1,0:T(4,128)(2,1)S(1)}, bf16[4,256]{1,0:T(4,128)(2,1)}, u32[]{:S(2)}) copy-start(bf16[4,256]{1,0:T(4,128)(2,1)} %q_ref.3) | copy-start | bytes 6148
  123.5 43.5 %all-to-all-start = ((bf16[32,24,256]{2,1,0:T(8,128)(2,1)}), bf16[32,24,256]{2,1,0:T(8,128)(2,1)S(1)}, u32[]{:S(2)}, u32[]{:S(2)}) async-start(bf16[32,24,256]{2,1,0:T(8,128)(2,1)} %bitcast), calls=%async_computation | async-start | bytes 786432 | tf_op jit(solution)/shard_map/all_to_all | solution.py:166
  128.3 1.9 copy-start
  167.0 39.3 %all-to-all-start.1 = ((f32[32,1,2176]{2,1,0:T(1,128)}), f32[32,1,2176]{2,1,0:T(1,128)S(1)}, u32[]{:S(2)}, u32[]{:S(2)}) async-start(f32[32,1,2176]{2,1,0:T(1,128)} %bitcast.4), calls=%async_computation.1 | async-start | bytes 557056 | tf_op jit(solution)/shard_map/all_to_all | solution.py:166
  173.5 13.7 %collective-permute-start = (bf16[768,256]{1,0:T(8,128)(2,1)S(1)}, bf16[768,256]{1,0:T(8,128)(2,1)S(1)}, u32[]{:S(2)}, u32[]{:S(2)}) collective-permute-start(bf16[768,256]{1,0:T(8,128)(2,1)S(1)} %bitcast.7), channel_id=1, source_target_pairs={{0,2},{1,3},{2,4},{3,5},{4,6},{5,7},{6,0},{7,1},{8,10},{9,11},{10,... | collective-permute-start | bytes 1179656 | tf_op jit(solution)/shard_map/ppermute | solution.py:171
  177.0 12.9 %collective-permute-start.1 = (bf16[768,256]{1,0:T(8,128)(2,1)S(1)}, bf16[768,256]{1,0:T(8,128)(2,1)S(1)}, u32[]{:S(2)}, u32[]{:S(2)}) collective-permute-start(bf16[768,256]{1,0:T(8,128)(2,1)S(1)} %bitcast.8), channel_id=1, source_target_pairs={{0,4},{1,5},{2,6},{3,7},{4,0},{5,1},{6,2},{7,3},{8,12},{9,13},{10,... | collective-permute-start | bytes 1179656 | tf_op jit(solution)/shard_map/ppermute | solution.py:171
  182.0 9.9 %collective-permute-start.2 = (bf16[768,256]{1,0:T(8,128)(2,1)S(1)}, bf16[768,256]{1,0:T(8,128)(2,1)}, u32[]{:S(2)}, u32[]{:S(2)}) collective-permute-start(bf16[768,256]{1,0:T(8,128)(2,1)S(1)} %bitcast.9), channel_id=1, source_target_pairs={{0,6},{1,7},{2,0},{3,1},{4,2},{5,3},{6,4},{7,5},{8,14},{9,15},{10,... | collective-permute-start | bytes 1179656 | tf_op jit(solution)/shard_map/ppermute | solution.py:171
  185.2 22.7 %collective-permute-start.3 = (bf16[768,256]{1,0:T(8,128)(2,1)S(1)}, bf16[768,256]{1,0:T(8,128)(2,1)}, u32[]{:S(2)}, u32[]{:S(2)}) collective-permute-start(bf16[768,256]{1,0:T(8,128)(2,1)S(1)} %bitcast.10), channel_id=1, source_target_pairs={{0,1},{1,0},{2,3},{3,2},{4,5},{5,4},{6,7},{7,6},{8,9},{9,8},{10,11... | collective-permute-start | bytes 1179656 | tf_op jit(solution)/shard_map/ppermute | solution.py:171
  187.2 20.7 %collective-permute-start.4 = (bf16[768,256]{1,0:T(8,128)(2,1)S(1)}, bf16[768,256]{1,0:T(8,128)(2,1)}, u32[]{:S(2)}, u32[]{:S(2)}) collective-permute-start(bf16[768,256]{1,0:T(8,128)(2,1)S(1)} %collective-permute-done.refs_1_), channel_id=1, source_target_pairs={{0,1},{1,0},{2,3},{3,2},{4,5},{5,4},{6,7},{7,6},{8,9},{9,8},{10,11... | collective-permute-start | bytes 1179656 | tf_op jit(solution)/shard_map/ppermute | solution.py:171
  190.0 18.0 %collective-permute-start.5 = (bf16[768,256]{1,0:T(8,128)(2,1)S(1)}, bf16[768,256]{1,0:T(8,128)(2,1)}, u32[]{:S(2)}, u32[]{:S(2)}) collective-permute-start(bf16[768,256]{1,0:T(8,128)(2,1)S(1)} %collective-permute-done.1.refs_2_), channel_id=1, source_target_pairs={{0,1},{1,0},{2,3},{3,2},{4,5},{5,4},{6,7},{7,6},{8,9},{9,8},{10,11... | collective-permute-start | bytes 1179656 | tf_op jit(solution)/shard_map/ppermute | solution.py:171
  191.9 16.0 %collective-permute-start.6 = (bf16[768,256]{1,0:T(8,128)(2,1)}, bf16[768,256]{1,0:T(8,128)(2,1)}, u32[]{:S(2)}, u32[]{:S(2)}) collective-permute-start(bf16[768,256]{1,0:T(8,128)(2,1)} %collective-permute-done.2.refs_3_), channel_id=1, source_target_pairs={{0,1},{1,0},{2,3},{3,2},{4,5},{5,4},{6,7},{7,6},{8,9},{9,8},{10,11... | collective-permute-start | bytes 1179656 | tf_op jit(solution)/shard_map/ppermute | solution.py:171
  194.4 3.1 %collective-permute-start.7 = (bf16[8,128]{1,0:T(8,128)(2,1)S(1)}, bf16[8,128]{1,0:T(8,128)(2,1)S(1)}, u32[]{:S(2)}, u32[]{:S(2)}) collective-permute-start(bf16[8,128]{1,0:T(8,128)(2,1)S(1)} %slice.3), channel_id=1, source_target_pairs={{0,1},{1,0},{2,3},{3,2},{4,5},{5,4},{6,7},{7,6},{8,9},{9,8},{10,11... | collective-permute-start | bytes 6152 | tf_op jit(solution)/shard_map/ppermute | solution.py:171
  197.5 0.7 copy-start.4
  198.2 0.7 copy-start.5
  198.8 0.7 copy-start.6
  199.5 0.7 copy-start.7
  200.2 0.7 copy-start.8
  201.6 0.6 copy-start.1
  206.3 0.7 copy-start.2

commit v5 on v3

--- a/solution.py
+++ b/solution.py
@@ -31,7 +31,7 @@
     return jnp.where(lane // HALF == slot, out, 0.0)
 
 
-def local_kernel(peers, heads, x_ref, w_ref, q_ref, part_ref):
+def local_kernel(heads, x_ref, w_ref, q_ref, pay_ref):
     count, piece, width = x_ref.shape
     rows = 2 * count * heads
     cols = heads * 2 * HALF
@@ -53,10 +53,12 @@
     part = jnp.zeros((rows, VDIM), F32)
     for h in range(heads):
         part = jnp.where(r % heads == h, full[:, h * VDIM : (h + 1) * VDIM], part)
-    stats = as_line([top, total])
-    for p in range(peers):
-        part_ref[p * (rows + 1) : p * (rows + 1) + rows, :] = part
-        part_ref[p * (rows + 1) + rows : (p + 1) * (rows + 1), :] = stats
+    part = part / total
+    power = jnp.ceil(jnp.log2(jnp.maximum(jnp.max(jnp.abs(part), axis=1, keepdims=True), 1e-30)))
+    pay_ref[:rows, :] = part * jnp.exp2(-power)
+    pay_ref[rows:, :] = jnp.zeros((pay_ref.shape[0] - rows, VDIM), F32)
+    pieces = [p.astype(F32) * 256.0**n for x in (top / 64, total) for n, p in enumerate(three(x))]
+    pay_ref[rows : rows + 1, :] = as_line([*pieces, power])
 
 
 def three(x):
@@ -92,18 +94,26 @@
             out_ref[n : n + 1, :] = values[b : b + 1, h * VDIM : (h + 1) * VDIM]
 
 
-def finish_kernel(peers, heads, part_ref, new_ref, out_ref):
+def row_of_each(part_ref, r):
+    each = part_ref.shape[2] // VDIM
+    return part_ref[r // each, :, (r % each) * VDIM : (r % each + 1) * VDIM]
+
+
+def finish_kernel(heads, part_ref, new_ref, out_ref):
     count = out_ref.shape[0]
     half = count * heads
     rows = 2 * half
     fresh = new_ref[0:1, :]
-    tops = part_ref[pl.ds(rows, peers, rows + 1), :]
-    totals = pltpu.roll(tops, VDIM - rows, 1)
+    stats = row_of_each(part_ref, rows)
+    piece = [pltpu.roll(stats, (VDIM - n * rows) % VDIM, 1) for n in range(7)]
+    tops = (piece[0] + piece[1] / 256.0 + piece[2] / 65536.0) * 64
+    totals = piece[3] + piece[4] / 256.0 + piece[5] / 65536.0
+    power = piece[6]
     top = jnp.maximum(jnp.max(tops, axis=0, keepdims=True), fresh)
-    scale = jnp.exp(tops - top)
+    scale = jnp.exp(jnp.minimum(tops - top, 0.0))
     own = jnp.exp(fresh - top)
     total = jnp.sum(totals * scale, axis=0, keepdims=True) + own
-    scale = scale * (new_ref[1:2, :] / total)
+    scale = scale * totals * jnp.exp2(power) * (new_ref[1:2, :] / total)
     own = own * (new_ref[1:2, :] / total)
     mine = (own + pltpu.roll(own, VDIM - half, 1)).astype(BF16).astype(F32)
     for b in range(count):
@@ -111,7 +121,7 @@
             n = b * heads + h
             reads = 0.0
             for r in (n, n + half):
-                reads += scale[:, r : r + 1] * part_ref[pl.ds(r, peers, rows + 1), :]
+                reads += scale[:, r : r + 1] * row_of_each(part_ref, r)
             reads = jnp.sum(reads, axis=0, keepdims=True)
             reads += mine[:, n : n + 1] * new_ref[8 + n : 9 + n, :]
             mean = jnp.mean(reads * reads, axis=1, keepdims=True)
@@ -198,12 +208,12 @@
         (mix_lambda, query_new, key_new, value_new, head_gain.reshape(1, VDIM)),
         "s",
     )
-    (parts,) = call(
-        functools.partial(local_kernel, peers, heads), [((peers * (2 * half + 1), VDIM), F32)], (prompt, w, query_new)
-    )
-    parts = parts.reshape(peers, 1, (2 * half + 1) * VDIM)
-    parts = spread(parts, "sp").reshape(peers * (2 * half + 1), VDIM)
-    (first_read,) = call(functools.partial(finish_kernel, peers, heads), [((count, cols), BF16)], (parts, fresh))
+    each = half + 1
+    (pay,) = call(functools.partial(local_kernel, heads), [((2 * each, VDIM), F32)], (prompt, w, query_new))
+    parts = jnp.broadcast_to(pay.reshape(2, each * VDIM).astype(jnp.float16), (peers, 2, each * VDIM))
+    parts = spread(parts, "sp")
+    parts = parts.astype(F32).transpose(1, 0, 2)
+    (first_read,) = call(functools.partial(finish_kernel, heads), [((count, cols), BF16)], (parts, fresh))
 
     found = [mine]
     for d in range(1, slices // 2):

time: 213 us -> 206 us (0.967)
  the two profiles are of different devices: /device:TPU:40 before, /device:TPU:46 now
where the time goes in v5:
time: 206 us
  blocking collectives  120 us (58%)
  waiting for transfers between devices  42.3 us (21%)
  starting transfers between devices  27.7 us (13%)
  Pallas kernels  8.96 us (4%)
  local copies, waits for them, and re-layouts  4.48 us (2%)
    all_gather x1, blocking collectives, inner(): w = lax.all_gather(w, 'sp', axis=0, tiled=True)  120 us
    all_to_all x2, waiting for transfers between devices, spread(): return lax.all_to_all(x, axis, 0, 0, tiled=True)  40.4 us
    ppermute x7, starting transfers between devices, moved(): return lax.ppermute(x, axis, [(i, step(i) % n) for i in range(n)])  16.9 us
    all_to_all x2, starting transfers between devices, spread(): return lax.all_to_all(x, axis, 0, 0, tiled=True)  10.8 us
    pallas_call x4, Pallas kernels, call(): pl.pallas_call(kernel, out_shape=[jax.ShapeDtypeStruct(s, d) for s, d in...  8.96 us
  transfers between devices with their start and end apart: 9, of which 3 were waited for; matrix products, arithmetic and copies ran while one was open for 0% of the time, Pallas kernels for 2%

profile of v5, /device:TPU:46, one launch (start us, length us, event | category | flops | bytes accessed | tf_op | source)
XLA Modules:
  0.0 205.5 jit_solution(15258919469345952003)
XLA Ops:
  0.6 1.8 constant_dynamic-slice_fusion
  2.4 0.8 multiply_convert_fusion.1
  3.2 0.0 copy-start.1
  3.2 119.9 %all-gather.1 = f16[2048,512]{1,0:T(8,128)(2,1)S(1)} all-gather(f16[64,512]{1,0:T(8,128)(2,1)S(1)} %multiply_convert_fusion.1), channel_id=1, replica_groups=mesh['grp'=2,'sp'=32,'tp'=8] {'sp'}, dimensions={0}, use_global_device_ids=true | all-gather | bytes 2162688 | tf_op jit(solution)/shard_map/all_gather | solution.py:200
  123.1 0.5 multiply_convert_fusion.refs_8_.w_ref
  123.6 0.0 copy-start.2
  123.6 0.0 copy-start.3
  123.6 0.0 copy-start.4
  123.7 0.0 copy-start.5
  123.7 4.9 %all-to-all-start = ((bf16[32,24,256]{2,1,0:T(8,128)(2,1)}), bf16[32,24,256]{2,1,0:T(8,128)(2,1)S(1)}, u32[]{:S(2)}, u32[]{:S(2)}) async-start(bf16[32,24,256]{2,1,0:T(8,128)(2,1)} %bitcast), calls=%async_computation | async-start | bytes 786432 | tf_op jit(solution)/shard_map/all_to_all | solution.py:176
  128.6 0.0 copy-start
  128.6 1.9 copy-done
  130.5 2.6 %shard_map.104 = f32[18,128]{1,0:T(8,128)S(1)} custom-call(bf16[4,192,2048]{2,1,0:T(8,128)(2,1)S(1)} %copy-done, bf16[2048,512]{1,0:T(8,128)(2,1)S(1)} %multiply_convert_fusion.refs_8_.w_ref, bf16[4,256]{1,0:T(4,128)(2,1)S(1)} %copy-done.1), custom_call_target="tpu_custom_call" | custom-call | tf_op jit(solution)/shard_map/pallas_call | solution.py:165
  133.2 32.8 %all-to-all-done = bf16[32,24,256]{2,1,0:T(8,128)(2,1)S(1)} async-done(((bf16[32,24,256]{2,1,0:T(8,128)(2,1)}), bf16[32,24,256]{2,1,0:T(8,128)(2,1)S(1)}, u32[]{:S(2)}, u32[]{:S(2)}) %all-to-all-start) | async-done | bytes 393248 | tf_op jit(solution)/shard_map/all_to_all | solution.py:176
  166.0 0.7 broadcast_in_dim.3
  166.7 5.9 %all-to-all-start.1 = ((f16[32,2,1152]{2,1,0:T(2,128)(2,1)}), f16[32,2,1152]{2,1,0:T(2,128)(2,1)S(1)}, u32[]{:S(2)}, u32[]{:S(2)}) async-start(f16[32,2,1152]{2,1,0:T(2,128)(2,1)} %broadcast_in_dim.3), calls=%async_computation.1 | async-start | bytes 294912 | tf_op jit(solution)/shard_map/all_to_all | solution.py:176
  172.6 2.0 collective-permute-start
  174.7 4.6 %collective-permute-start.1 = (bf16[768,256]{1,0:T(8,128)(2,1)S(1)}, bf16[768,256]{1,0:T(8,128)(2,1)S(1)}, u32[]{:S(2)}, u32[]{:S(2)}) collective-permute-start(bf16[768,256]{1,0:T(8,128)(2,1)S(1)} %bitcast.8), channel_id=1, source_target_pairs={{0,4},{1,5},{2,6},{3,7},{4,0},{5,1},{6,2},{7,3},{8,12},{9,13},{10,... | collective-permute-start | bytes 1179656 | tf_op jit(solution)/shard_map/ppermute | solution.py:181
  179.3 2.0 collective-permute-start.2
  181.3 0.8 shard_map.105.new_ref
  182.1 2.0 collective-permute-start.3
  184.0 0.0 collective-permute-done.refs_1_
  184.0 2.4 %collective-permute-start.4 = (bf16[768,256]{1,0:T(8,128)(2,1)S(1)}, bf16[768,256]{1,0:T(8,128)(2,1)}, u32[]{:S(2)}, u32[]{:S(2)}) collective-permute-start(bf16[768,256]{1,0:T(8,128)(2,1)S(1)} %collective-permute-done.refs_1_), channel_id=1, source_target_pairs={{0,1},{1,0},{2,3},{3,2},{4,5},{5,4},{6,7},{7,6},{8,9},{9,8},{10,11... | collective-permute-start | bytes 1179656 | tf_op jit(solution)/shard_map/ppermute | solution.py:181
  186.5 0.0 collective-permute-done.1.refs_2_
  186.5 2.0 collective-permute-start.5
  188.5 1.9 collective-permute-done.2.refs_3_
  190.3 1.9 collective-permute-start.6
  192.3 7.6 %all-to-all-done.1 = f16[32,2,1152]{2,1,0:T(2,128)(2,1)S(1)} async-done(((f16[32,2,1152]{2,1,0:T(2,128)(2,1)}), f16[32,2,1152]{2,1,0:T(2,128)(2,1)S(1)}, u32[]{:S(2)}, u32[]{:S(2)}) %all-to-all-start.1) | async-done | bytes 147488 | tf_op jit(solution)/shard_map/all_to_all | solution.py:176
  199.9 1.0 shard_map.106
  200.9 0.0 collective-permute-done.3.refs_4_
  200.9 0.0 collective-permute-done.6.refs_7_
  200.9 4.6 %shard_map.103 = (bf16[768,256]{1,0:T(8,128)(2,1)}, bf16[768,256]{1,0:T(8,128)(2,1)}) custom-call(bf16[768,256]{1,0:T(8,128)(2,1)S(1)} %bitcast.11, bf16[768,256]{1,0:T(8,128)(2,1)S(1)} %collective-permute-done.refs_1_, bf16[768,256]{1,0:T(8,128)(2,1)S(1)} %collective-permute-done.1.refs_2_, bf16[768,256]{1,0:T(8,128)(2,1)} %collective-permute-done.2.refs_3_, ...), custom_call_target="tpu_custom_call" | custom-call | tf_op jit(solution)/shard_map/pallas_call | solution.py:165
  (10 shorter events, 0.1 us)
Async XLA Ops:
  3.2 125.4 %copy-start.1 = (bf16[4,256]{1,0:T(4,128)(2,1)S(1)}, bf16[4,256]{1,0:T(4,128)(2,1)}, u32[]{:S(2)}) copy-start(bf16[4,256]{1,0:T(4,128)(2,1)} %q_ref.3) | copy-start | bytes 6148
  123.6 57.6 %copy-start.2 = (bf16[4,256]{1,0:T(4,128)(2,1)S(1)}, bf16[4,256]{1,0:T(4,128)(2,1)}, u32[]{:S(2)}) copy-start(bf16[4,256]{1,0:T(4,128)(2,1)} %kn_ref.1) | copy-start | bytes 6148
  123.6 57.6 %copy-start.3 = (bf16[4,256]{1,0:T(4,128)(2,1)S(1)}, bf16[4,256]{1,0:T(4,128)(2,1)}, u32[]{:S(2)}) copy-start(bf16[4,256]{1,0:T(4,128)(2,1)} %vn_ref.1) | copy-start | bytes 6148
  123.6 57.6 %copy-start.4 = (f32[2]{0:T(128)S(1)}, f32[2]{0:T(128)}, u32[]{:S(2)}) copy-start(f32[2]{0:T(128)} %lam_ref.1) | copy-start | bytes 28
  123.7 57.6 %copy-start.5 = (f32[128]{0:T(128)S(1)}, f32[128]{0:T(128)}, u32[]{:S(2)}) copy-start(f32[128]{0:T(128)} %param.15) | copy-start | bytes 1540
  123.7 42.3 %all-to-all-start = ((bf16[32,24,256]{2,1,0:T(8,128)(2,1)}), bf16[32,24,256]{2,1,0:T(8,128)(2,1)S(1)}, u32[]{:S(2)}, u32[]{:S(2)}) async-start(bf16[32,24,256]{2,1,0:T(8,128)(2,1)} %bitcast), calls=%async_computation | async-start | bytes 786432 | tf_op jit(solution)/shard_map/all_to_all | solution.py:176
  128.6 1.9 copy-start
  166.7 33.2 %all-to-all-start.1 = ((f16[32,2,1152]{2,1,0:T(2,128)(2,1)}), f16[32,2,1152]{2,1,0:T(2,128)(2,1)S(1)}, u32[]{:S(2)}, u32[]{:S(2)}) async-start(f16[32,2,1152]{2,1,0:T(2,128)(2,1)} %broadcast_in_dim.3), calls=%async_computation.1 | async-start | bytes 294912 | tf_op jit(solution)/shard_map/all_to_all | solution.py:176
  172.6 11.4 %collective-permute-start = (bf16[768,256]{1,0:T(8,128)(2,1)S(1)}, bf16[768,256]{1,0:T(8,128)(2,1)S(1)}, u32[]{:S(2)}, u32[]{:S(2)}) collective-permute-start(bf16[768,256]{1,0:T(8,128)(2,1)S(1)} %bitcast.7), channel_id=1, source_target_pairs={{0,2},{1,3},{2,4},{3,5},{4,6},{5,7},{6,0},{7,1},{8,10},{9,11},{10,... | collective-permute-start | bytes 1179656 | tf_op jit(solution)/shard_map/ppermute | solution.py:181
  174.7 11.8 %collective-permute-start.1 = (bf16[768,256]{1,0:T(8,128)(2,1)S(1)}, bf16[768,256]{1,0:T(8,128)(2,1)S(1)}, u32[]{:S(2)}, u32[]{:S(2)}) collective-permute-start(bf16[768,256]{1,0:T(8,128)(2,1)S(1)} %bitcast.8), channel_id=1, source_target_pairs={{0,4},{1,5},{2,6},{3,7},{4,0},{5,1},{6,2},{7,3},{8,12},{9,13},{10,... | collective-permute-start | bytes 1179656 | tf_op jit(solution)/shard_map/ppermute | solution.py:181
  179.3 11.0 %collective-permute-start.2 = (bf16[768,256]{1,0:T(8,128)(2,1)S(1)}, bf16[768,256]{1,0:T(8,128)(2,1)}, u32[]{:S(2)}, u32[]{:S(2)}) collective-permute-start(bf16[768,256]{1,0:T(8,128)(2,1)S(1)} %bitcast.9), channel_id=1, source_target_pairs={{0,6},{1,7},{2,0},{3,1},{4,2},{5,3},{6,4},{7,5},{8,14},{9,15},{10,... | collective-permute-start | bytes 1179656 | tf_op jit(solution)/shard_map/ppermute | solution.py:181
  182.1 18.8 %collective-permute-start.3 = (bf16[768,256]{1,0:T(8,128)(2,1)S(1)}, bf16[768,256]{1,0:T(8,128)(2,1)}, u32[]{:S(2)}, u32[]{:S(2)}) collective-permute-start(bf16[768,256]{1,0:T(8,128)(2,1)S(1)} %bitcast.10), channel_id=1, source_target_pairs={{0,1},{1,0},{2,3},{3,2},{4,5},{5,4},{6,7},{7,6},{8,9},{9,8},{10,11... | collective-permute-start | bytes 1179656 | tf_op jit(solution)/shard_map/ppermute | solution.py:181
  184.0 16.9 %collective-permute-start.4 = (bf16[768,256]{1,0:T(8,128)(2,1)S(1)}, bf16[768,256]{1,0:T(8,128)(2,1)}, u32[]{:S(2)}, u32[]{:S(2)}) collective-permute-start(bf16[768,256]{1,0:T(8,128)(2,1)S(1)} %collective-permute-done.refs_1_), channel_id=1, source_target_pairs={{0,1},{1,0},{2,3},{3,2},{4,5},{5,4},{6,7},{7,6},{8,9},{9,8},{10,11... | collective-permute-start | bytes 1179656 | tf_op jit(solution)/shard_map/ppermute | solution.py:181
  186.5 14.4 %collective-permute-start.5 = (bf16[768,256]{1,0:T(8,128)(2,1)S(1)}, bf16[768,256]{1,0:T(8,128)(2,1)}, u32[]{:S(2)}, u32[]{:S(2)}) collective-permute-start(bf16[768,256]{1,0:T(8,128)(2,1)S(1)} %collective-permute-done.1.refs_2_), channel_id=1, source_target_pairs={{0,1},{1,0},{2,3},{3,2},{4,5},{5,4},{6,7},{7,6},{8,9},{9,8},{10,11... | collective-permute-start | bytes 1179656 | tf_op jit(solution)/shard_map/ppermute | solution.py:181
  190.3 10.6 %collective-permute-start.6 = (bf16[768,256]{1,0:T(8,128)(2,1)}, bf16[768,256]{1,0:T(8,128)(2,1)}, u32[]{:S(2)}, u32[]{:S(2)}) collective-permute-start(bf16[768,256]{1,0:T(8,128)(2,1)} %collective-permute-done.2.refs_3_), channel_id=1, source_target_pairs={{0,1},{1,0},{2,3},{3,2},{4,5},{5,4},{6,7},{7,6},{8,9},{9,8},{10,11... | collective-permute-start | bytes 1179656 | tf_op jit(solution)/shard_map/ppermute | solution.py:181
